TPU v7x, 256 devices: a whole 4x4x8 slice. The times are simulated.
256 devices in a mesh: vp: 16 (over y, x), dp: 16 (over z, core).
Axes of the slice: x: 4, y: 4, z: 8, core: 2. Of those that a mesh axis runs over, the one named last changes fastest.
Arguments:
- hidden_act: bfloat16 [8192, 8192], P('dp', 'vp'), may hold values from 0 to 36
- down_weight: bfloat16 [8192, 2048], P('vp'), may hold values from -0.0625 to 0.0625
- residual: bfloat16 [8192, 2048], P(('dp', 'vp')), may hold values from -300 to 300
- post_gain: float32 [2048], replicated, may hold values from 0.1 to 1.9
- final_gain: float32 [2048], replicated, may hold values from 0.1 to 1.9
- vocab: bfloat16 [2048, 32768], P(None, 'vp'), may hold values from -0.33 to 0.33
- vocab_bias: float32 [32768], P('vp'), may hold values from -2.5 to 2.5
- target_ids: int32 [8192, 4], P('dp'), may hold values from 0 to 32767
- target_weights: float32 [8192, 4], P('dp'), may hold values from 0 to 1, as said below
Outputs:
- losses: float32 [8192], P(('dp', 'vp'))
- stream_grad: float32 [8192, 2048], P(('dp', 'vp'))
- vocab_grad: float32 [2048, 32768], P('dp', 'vp')
Inputs may be any that keep to these rules, and one draw needn't show every extreme that they name: `target_weights`: the 4 weights of a token add up to one.
All inputs are finite; a program needn't handle non-finite values.
Results may differ from a plain program's by a relative error of at most 0.01225.
Values may be sent and summed in bfloat16 or wider, within the bound.
A program may use at most 128 MiB of HBM per device.

v0:
```python
import jax
import jax.numpy as jnp
from jax import lax
from jax.sharding import Mesh
from jax.sharding import PartitionSpec as P

COL_BLOCK = 512
VP = ("vp_0", "vp_1")
DP_VP = ("dp", "vp_0", "vp_1")


epsilon = 1e-06
z_weight = 0.001
loss_scale = 32.0


def sum_by_axis(so_far, axes):
    for axis in axes:
        so_far = lax.psum_scatter(so_far, axis, scatter_dimension=0, tiled=True)
    return so_far


def copy_for_each(x, axis):
    copies = jnp.broadcast_to(x, (lax.axis_size(axis), *x.shape))
    return lax.all_to_all(copies, axis, split_axis=0, concat_axis=0, tiled=True)


def in_order(parts, dim):
    parts = jnp.moveaxis(parts, 0, dim)
    shape = parts.shape
    return parts.reshape(*shape[:dim], shape[dim] * shape[dim + 1], *shape[dim + 2 :])


def gather_directly(x, axis, dim):
    parts = copy_for_each(x, axis)
    return in_order(parts, dim)


def collected_together(x, axis):
    leaves = jax.tree.leaves(x)
    turns = sorted(range(len(leaves)), key=lambda k: -leaves[k].size)
    width = (1, *leaves[turns[0]].shape)[-1]
    lines = [
        jnp.pad(leaves[k].reshape(-1), (0, -leaves[k].size % width)).reshape(-1, width)
        for k in turns
    ]
    both, at, found = (copy_for_each(jnp.concatenate(lines), axis), 0, {})
    for k, line in zip(turns, lines):
        share = both[:, at : at + len(line)].reshape(len(both), -1)
        found[k] = share[:, : leaves[k].size].reshape(-1, *leaves[k].shape)
        at += len(line)
    numbers = iter(range(len(leaves)))
    return jax.tree.map(lambda _: found[next(numbers)], x)


def combined_pairwise(pieces, combine):
    while len(jax.tree.leaves(pieces)[0]) > 1:
        pieces = jax.vmap(combine)(
            *(jax.tree.map(lambda part: part[side::2], pieces) for side in (0, 1))
        )
    return jax.tree.map(lambda part: part[0], pieces)


def joined_all(x, axis, combine):
    pieces = collected_together(x, axis)
    return combined_pairwise(pieces, combine)


def split_up(x, dim, size):
    shape = x.shape
    parts = x.reshape(*shape[:dim], size, shape[dim] // size, *shape[dim + 1 :])
    return jnp.moveaxis(parts, dim, 0)


def sent_and_summed(x, axis, dim):
    parts = split_up(x, dim, lax.axis_size(axis))
    arrived = lax.all_to_all(parts, axis, split_axis=0, concat_axis=0, tiled=True)
    return arrived.sum(axis=0)


def inverse_rms(values):
    return lax.rsqrt(jnp.mean(values * values, axis=-1, keepdims=True) + epsilon)


def combine_stats(first_stats, second_stats):
    joint_max = jnp.maximum(first_stats[0], second_stats[0])
    joint_sum = first_stats[1] * jnp.exp(first_stats[0] - joint_max) + second_stats[1] * jnp.exp(
        second_stats[0] - joint_max
    )
    return (joint_max, joint_sum, first_stats[2] + second_stats[2])


def shards(
    hidden_act,
    down_weight,
    residual,
    post_gain,
    final_gain,
    vocab,
    vocab_bias,
    target_ids,
    target_weights,
):
    own_rows = residual.shape[0]
    group_rows = hidden_act.shape[0]
    width = vocab.shape[0]
    columns = vocab.shape[1]
    blocks = columns // COL_BLOCK
    vp_index = lax.axis_index(VP)
    branch = sum_by_axis(jnp.dot(hidden_act, down_weight, preferred_element_type=jnp.float32), VP)
    stream = residual.astype(jnp.float32) + branch * inverse_rms(branch) * post_gain
    inverse = inverse_rms(stream)
    normed = (stream * inverse * final_gain).astype(jnp.bfloat16)
    gathered = gather_directly(normed, VP, 0)
    local_ids = target_ids - vp_index * columns
    vocab_split = vocab.reshape(width, blocks, COL_BLOCK)
    bias_split = vocab_bias.reshape(blocks, COL_BLOCK)

    def block_wanted(block_index):
        position = block_index * COL_BLOCK + lax.broadcasted_iota(jnp.int32, (1, COL_BLOCK), 1)
        wanted = jnp.zeros((group_rows, COL_BLOCK), jnp.float32)
        for target_k in range(target_ids.shape[1]):
            wanted = wanted + jnp.where(
                local_ids[:, target_k : target_k + 1] == position,
                target_weights[:, target_k : target_k + 1],
                0.0,
            )
        return wanted

    def gather_stats(running, block_index):
        run_max, run_sum, run_target = running
        weight_block = lax.dynamic_index_in_dim(vocab_split, block_index, 1, keepdims=False)
        bias_block = lax.dynamic_index_in_dim(bias_split, block_index, 0, keepdims=False)
        scores = jnp.dot(gathered, weight_block, preferred_element_type=jnp.float32) + bias_block
        wanted = block_wanted(block_index)
        new_max = jnp.maximum(run_max, jnp.max(scores, axis=1))
        run_sum = run_sum * jnp.exp(run_max - new_max) + jnp.sum(
            jnp.exp(scores - new_max[:, None]), axis=1
        )
        run_target = run_target + jnp.sum(wanted * scores, axis=1)
        return ((new_max, run_sum, run_target), scores)

    zeros_rows = jnp.zeros((group_rows,), jnp.float32)
    start_stats = (jnp.full((group_rows,), -jnp.inf, jnp.float32), zeros_rows, zeros_rows)
    local_stats, stored_scores = lax.scan(gather_stats, start_stats, jnp.arange(blocks))
    local_max, local_sum, local_target = local_stats
    row_max, row_sum, target_score = joined_all(
        (local_max, local_sum, local_target), VP, combine_stats
    )
    log_norm = row_max + jnp.log(row_sum)
    group_losses = log_norm - target_score + z_weight * log_norm * log_norm
    losses = lax.dynamic_slice_in_dim(group_losses, vp_index * own_rows, own_rows, 0)
    factor = (1.0 + 2.0 * z_weight * log_norm)[:, None]

    def score_grad(inputs):
        block_index, scores = inputs
        probability = jnp.exp(scores - log_norm[:, None])
        return (loss_scale * (probability * factor - block_wanted(block_index))).astype(
            jnp.bfloat16
        )

    score_grads = lax.map(score_grad, (jnp.arange(blocks), stored_scores))
    row_grad = sent_and_summed(
        jnp.einsum("jrc,djc->rd", score_grads, vocab_split, preferred_element_type=jnp.float32),
        VP,
        0,
    )
    slice_width = width // lax.axis_size("dp")
    vocab_grad = lax.psum_scatter(
        jnp.einsum("rd,jrc->djc", gathered, score_grads, preferred_element_type=jnp.float32)
        .reshape(lax.axis_size("dp") * slice_width, columns)
        .astype(jnp.bfloat16),
        "dp",
        scatter_dimension=0,
        tiled=True,
    ).astype(jnp.float32)
    upstream = row_grad * final_gain
    stream_grad = inverse * (
        upstream - stream * inverse * inverse * jnp.mean(upstream * stream, axis=-1, keepdims=True)
    )
    return (losses, stream_grad, vocab_grad)


def solution(mesh):
    split = Mesh(mesh.devices.reshape(4, 4, mesh.shape["dp"]), ("vp_0", "vp_1", "dp"))
    placed = (
        P("dp", VP),
        P(VP, None),
        P(DP_VP, None),
        P(),
        P(),
        P(None, VP),
        P(VP),
        P("dp", None),
        P("dp", None),
    )
    return jax.shard_map(
        shards,
        mesh=split,
        in_specs=placed,
        out_specs=(P(DP_VP), P(DP_VP, None), P("dp", VP)),
        check_vma=False,
    )
```

profile of v0, /device:TPU:2, one launch (start us, length us, event | category | flops | bytes accessed | tf_op | source)
XLA Modules:
  0.0 302.9 jit_solution(13956063655695743017)
XLA Ops:
  7.2 1.5 copy-done
  8.8 4.2 %fusion.21 = f32[512,2048]{1,0:T(8,128)} fusion(bf16[512,512]{1,0:T(8,128)(2,1)} %param.13, bf16[512,2048]{1,0:T(8,128)(2,1)S(1)} %copy-done), kind=kOutput, calls=%fused_computation.56 | convolution fusion | flops 1073741824 | bytes 6815744 | tf_op jit(solution)/shard_map/dot_general | solution.py:110
  13.1 52.5 %reduce-scatter.4.cloned.1.call-done = f32[128,2048]{1,0:T(8,128)} async-done(((f32[512,2048]{1,0:T(8,128)}), f32[128,2048]{1,0:T(8,128)}) %reduce-scatter.4.cloned.1.call-update) | async-done | bytes 1048592 | tf_op jit(solution)/shard_map/reduce_scatter | solution.py:19
  65.6 26.4 %reduce-scatter.6.cloned.1.call-done = f32[32,2048]{1,0:T(8,128)} async-done(((f32[128,2048]{1,0:T(8,128)}), f32[32,2048]{1,0:T(8,128)}) %reduce-scatter.6.cloned.1.call-update) | async-done | bytes 262160 | tf_op jit(solution)/shard_map/reduce_scatter | solution.py:19
  92.0 1.1 multiply_reduce_fusion.2
  93.1 1.2 multiply_reduce_fusion.1
  94.3 1.1 multiply_convert_fusion.1
  95.4 1.6 broadcast_in_dim.109
  96.9 8.0 %all-to-all-start = ((bf16[16,32,2048]{2,1,0:T(8,128)(2,1)}), bf16[16,32,2048]{2,1,0:T(8,128)(2,1)}, u32[]{:S(2)}, u32[]{:S(2)}) async-start(bf16[16,32,2048]{2,1,0:T(8,128)(2,1)} %broadcast_in_dim.109), calls=%async_computation.2 | async-start | bytes 4194304 | tf_op jit(solution)/shard_map/all_to_all | solution.py:25
  105.0 12.4 %copy.20 = bf16[2048,2048]{0,1:T(8,128)(2,1)} copy(bf16[2048,2048]{1,0:T(8,128)(2,1)} %param.18) | data formatting | bytes 16777216 | tf_op args[5]
  117.4 13.2 %all-to-all-done = bf16[16,32,2048]{2,1,0:T(8,128)(2,1)} async-done(((bf16[16,32,2048]{2,1,0:T(8,128)(2,1)}), bf16[16,32,2048]{2,1,0:T(8,128)(2,1)}, u32[]{:S(2)}, u32[]{:S(2)}) %all-to-all-start) | async-done | bytes 2097184 | tf_op jit(solution)/shard_map/all_to_all | solution.py:25
  130.6 34.1 %while.28 = (s32[]{:T(128)}, f32[512]{0:T(512)S(1)}, f32[512]{0:T(512)S(1)}, f32[512]{0:T(512)S(1)}, f32[4,512,512]{1,2,0:T(8,128)}, /*index=5*/s32[4]{0:T(128)S...) while((s32[]{:T(128)}, f32[512]{0:T(512)S(1)}, ...), condition=%wide.region_8.9_spmd.clone, body=%wide.region_4.8_spmd.clone.sunk | while | flops 1078201856 | bytes 8483050 | solution.py:145
  133.2 3.5 %fusion.41 = (f32[512]{0:T(512)S(1)}, f32[512,512]{1,0:T(8,128)S(1)}) fusion(f32[512]{0:T(512)S(1)} %bitcast.150, bf16[512,2048]{1,0:T(8,128)(2,1)} %get-tuple-element.451, bf16[2048,4,512]{0,2,1:T(8,128)(2,1)} %get-tuple-element.450, s32[]{:T(128)S(6)} %select_n.101), kind=kOutput, calls=%fused_computation.54.clone.1 | convolution fusion | flops 1074265600 | bytes 5246980 | tf_op jit(solution)/shard_map/while/body/eval_jaxpr/dot_general | solution.py:134
  137.4 0.7 fusion.44
  138.1 1.1 bitcast_dynamic-update-slice_fusion.2
  141.7 3.5 %fusion.41 = (f32[512]{0:T(512)S(1)}, f32[512,512]{1,0:T(8,128)S(1)}) fusion(f32[512]{0:T(512)S(1)} %bitcast.150, bf16[512,2048]{1,0:T(8,128)(2,1)} %get-tuple-element.451, bf16[2048,4,512]{0,2,1:T(8,128)(2,1)} %get-tuple-element.450, s32[]{:T(128)S(6)} %select_n.101), kind=kOutput, calls=%fused_computation.54.clone.1 | convolution fusion | flops 1074265600 | bytes 5246980 | tf_op jit(solution)/shard_map/while/body/eval_jaxpr/dot_general | solution.py:134
  146.0 0.7 fusion.44
  146.7 1.0 bitcast_dynamic-update-slice_fusion.2
  150.2 3.5 %fusion.41 = (f32[512]{0:T(512)S(1)}, f32[512,512]{1,0:T(8,128)S(1)}) fusion(f32[512]{0:T(512)S(1)} %bitcast.150, bf16[512,2048]{1,0:T(8,128)(2,1)} %get-tuple-element.451, bf16[2048,4,512]{0,2,1:T(8,128)(2,1)} %get-tuple-element.450, s32[]{:T(128)S(6)} %select_n.101), kind=kOutput, calls=%fused_computation.54.clone.1 | convolution fusion | flops 1074265600 | bytes 5246980 | tf_op jit(solution)/shard_map/while/body/eval_jaxpr/dot_general | solution.py:134
  154.5 0.7 fusion.44
  155.2 1.1 bitcast_dynamic-update-slice_fusion.2
  158.8 3.5 %fusion.41 = (f32[512]{0:T(512)S(1)}, f32[512,512]{1,0:T(8,128)S(1)}) fusion(f32[512]{0:T(512)S(1)} %bitcast.150, bf16[512,2048]{1,0:T(8,128)(2,1)} %get-tuple-element.451, bf16[2048,4,512]{0,2,1:T(8,128)(2,1)} %get-tuple-element.450, s32[]{:T(128)S(6)} %select_n.101), kind=kOutput, calls=%fused_computation.54.clone.1 | convolution fusion | flops 1074265600 | bytes 5246980 | tf_op jit(solution)/shard_map/while/body/eval_jaxpr/dot_general | solution.py:134
  163.0 0.7 fusion.44
  163.7 1.1 bitcast_dynamic-update-slice_fusion.2
  164.8 0.7 broadcast_in_dim.110
  165.4 6.7 %all-to-all-start.1 = ((f32[16,3,512]{2,1,0:T(4,128)}), f32[16,3,512]{2,1,0:T(4,128)S(1)}, u32[]{:S(2)}, u32[]{:S(2)}) async-start(f32[16,3,512]{2,1,0:T(4,128)} %broadcast_in_dim.110), calls=%async_computation.3 | async-start | bytes 262144 | tf_op jit(solution)/shard_map/all_to_all | solution.py:25
  172.4 6.5 %all-to-all-done.1 = f32[16,3,512]{2,1,0:T(4,128)S(1)} async-done(((f32[16,3,512]{2,1,0:T(4,128)}), f32[16,3,512]{2,1,0:T(4,128)S(1)}, u32[]{:S(2)}, u32[]{:S(2)}) %all-to-all-start.1) | async-done | bytes 98336 | tf_op jit(solution)/shard_map/all_to_all | solution.py:25
  179.3 26.9 %while.27 = (s32[]{:T(128)}, bf16[4,512,512]{2,1,0:T(8,128)(2,1)}, f32[4,512,512]{1,2,0:T(8,128)}, f32[512]{0:T(512)S(1)}, f32[512,1]{0,1:T(1,128)S(1)}, /*index...) while((s32[]{:T(128)}, bf16[4,512,512]{2,1,0:T(8,128)(2,1)}, ...), condition=%wide.region_10.11_spmd, body=%wide.region_9.10_spmd.sunk | while | flops 4194819 | bytes 5824657 | solution.py:162
  179.3 2.3 constant_dynamic-slice_fusion.4
  181.6 1.6 copy.39
  184.4 1.6 fusion.39
  186.1 2.3 constant_dynamic-slice_fusion.4
  188.3 1.6 copy.39
  191.2 1.6 fusion.39
  192.8 2.3 constant_dynamic-slice_fusion.4
  195.0 1.6 copy.39
  197.9 1.6 fusion.39
  199.5 2.3 constant_dynamic-slice_fusion.4
  201.8 1.6 copy.39
  204.6 1.6 fusion.39
  206.2 4.1 %copy.25 = bf16[4,512,512]{1,2,0:T(8,128)(2,1)} copy(bf16[4,512,512]{2,1,0:T(8,128)(2,1)} %get-tuple-element.109) | data formatting | bytes 4194304 | tf_op jit(solution)/shard_map/while | solution.py:162
  210.4 10.0 %convolution_convert_fusion = bf16[2048,2048]{1,0:T(8,128)(2,1)} fusion(bf16[512,2048]{1,0:T(8,128)(2,1)} %bitcast.11, bf16[2048,512]{1,0:T(8,128)(2,1)} %bitcast.126), kind=kOutput, calls=%fused_computation.21 | convolution fusion | flops 4299161600 | bytes 12582912 | tf_op jit(solution)/shard_map/rd,jrc->djc/dot_general | solution.py:170
  220.4 10.4 %convolution_bitcast_fusion = f32[16,32,2048]{2,1,0:T(8,128)} fusion(bf16[16,32,512,4]{2,1,0,3:T(8,128)(2,1)} %bitcast.125, bf16[2048,4,512,1]{0,2,3,1:T(8,128)(2,1)} %bitcast.124), kind=kOutput, calls=%fused_computation.22 | convolution fusion | flops 4294967296 | bytes 14680064 | tf_op jit(solution)/shard_map/jrc,djc->rd/dot_general | solution.py:164
  230.9 5.7 %all-to-all-start.2 = ((f32[16,32,2048]{2,1,0:T(8,128)}), f32[16,32,2048]{2,1,0:T(8,128)}, u32[]{:S(2)}, u32[]{:S(2)}) async-start(f32[16,32,2048]{2,1,0:T(8,128)} %convolution_bitcast_fusion), calls=%async_computation.4 | async-start | bytes 8388608 | tf_op jit(solution)/shard_map/all_to_all | solution.py:77
  237.4 53.3 %all-to-all-done.2 = f32[16,32,2048]{2,1,0:T(8,128)} async-done(((f32[16,32,2048]{2,1,0:T(8,128)}), f32[16,32,2048]{2,1,0:T(8,128)}, u32[]{:S(2)}, u32[]{:S(2)}) %all-to-all-start.2) | async-done | bytes 4194336 | tf_op jit(solution)/shard_map/all_to_all | solution.py:77
  290.6 2.5 reduce_sum.56
  293.4 0.9 subtract_multiply_fusion
  294.2 2.1 convert_element_type.19
  (115 shorter events, 6.9 us)
Async XLA Ops:
  7.2 1.6 copy-start
  7.2 58.4 %reduce-scatter.4.cloned.1.call-start = ((), (), s32[]{:S(2)}) async-start(), calls=%async_computation.6 | async-start | bytes 5242880 | tf_op jit(solution)/shard_map/reduce_scatter | solution.py:19
  13.0 80.1 %copy-start.2 = (bf16[32,2048]{1,0:T(8,128)(2,1)S(1)}, bf16[32,2048]{1,0:T(8,128)(2,1)}, u32[]{:S(2)}) copy-start(bf16[32,2048]{1,0:T(8,128)(2,1)} %param.15) | copy-start | bytes 393220
  13.0 80.1 %copy-start.4 = (f32[2048]{0:T(1024)S(1)}, f32[2048]{0:T(1024)}, u32[]{:S(2)}) copy-start(f32[2048]{0:T(1024)} %param.16) | copy-start | bytes 24580
  13.0 81.3 %copy-start.5 = (f32[2048]{0:T(1024)S(1)}, f32[2048]{0:T(1024)}, u32[]{:S(2)}) copy-start(f32[2048]{0:T(1024)} %param.17) | copy-start | bytes 24580
  13.0 78.9 %reduce-scatter.6.cloned.1.call-start = ((), (), s32[]{:S(2)}) async-start(), calls=%async_computation.7 | async-start | bytes 1310720 | tf_op jit(solution)/shard_map/reduce_scatter | solution.py:19
  96.9 33.7 %all-to-all-start = ((bf16[16,32,2048]{2,1,0:T(8,128)(2,1)}), bf16[16,32,2048]{2,1,0:T(8,128)(2,1)}, u32[]{:S(2)}, u32[]{:S(2)}) async-start(bf16[16,32,2048]{2,1,0:T(8,128)(2,1)} %broadcast_in_dim.109), calls=%async_computation.2 | async-start | bytes 4194304 | tf_op jit(solution)/shard_map/all_to_all | solution.py:25
  104.9 12.4 %copy-start.6 = (f32[2048]{0:T(1024)S(1)}, f32[2048]{0:T(1024)}, u32[]{:S(2)}) copy-start(f32[2048]{0:T(1024)} %param.19) | copy-start | bytes 24580
  105.0 12.4 %copy-start.7 = (s32[512,4]{0,1:T(4,128)S(1)}, s32[512,4]{0,1:T(4,128)}, u32[]{:S(2)}) copy-start(s32[512,4]{0,1:T(4,128)} %param.20) | copy-start | bytes 24580
  105.0 25.6 %copy-start.3 = (f32[512,4]{0,1:T(4,128)S(1)}, f32[512,4]{0,1:T(4,128)}, u32[]{:S(2)}) copy-start(f32[512,4]{0,1:T(4,128)} %param.21) | copy-start | bytes 24580
  165.4 13.4 %all-to-all-start.1 = ((f32[16,3,512]{2,1,0:T(4,128)}), f32[16,3,512]{2,1,0:T(4,128)S(1)}, u32[]{:S(2)}, u32[]{:S(2)}) async-start(f32[16,3,512]{2,1,0:T(4,128)} %broadcast_in_dim.110), calls=%async_computation.3 | async-start | bytes 262144 | tf_op jit(solution)/shard_map/all_to_all | solution.py:25
  172.1 122.1 %reduce-scatter.8.cloned.1.call-start = ((), (), s32[]{:S(2)}) async-start(), calls=%async_computation.8 | async-start | bytes 8912896 | tf_op jit(solution)/shard_map/reduce_scatter | solution.py:169
  230.9 59.8 %all-to-all-start.2 = ((f32[16,32,2048]{2,1,0:T(8,128)}), f32[16,32,2048]{2,1,0:T(8,128)}, u32[]{:S(2)}, u32[]{:S(2)}) async-start(f32[16,32,2048]{2,1,0:T(8,128)} %convolution_bitcast_fusion), calls=%async_computation.4 | async-start | bytes 8388608 | tf_op jit(solution)/shard_map/all_to_all | solution.py:77
  237.4 55.8 %copy-start.1 = (f32[32,2048]{1,0:T(8,128)S(1)}, f32[32,2048]{1,0:T(8,128)}, u32[]{:S(2)}) copy-start(f32[32,2048]{1,0:T(8,128)} %reduce-scatter.6.cloned.1.call-done) | copy-start | bytes 786436
Sparse Core Ops, SparseCore 0:
  13.1 52.3 reduce-scatter.3
  68.1 23.8 reduce-scatter.5
  220.5 71.1 reduce-scatter.7
where the time goes:
time: 309 us; the launch traced here: 303 us
  waiting for transfers between devices  152 us (49%)
  local copies, waits for them, and re-layouts  45.8 us (15%)
  matrix products  38.8 us (13%)
  starting transfers between devices  20.7 us (7%)
  other arithmetic  18.4 us (6%)
  between operations  14 us (5%)
  loops' own time  13.3 us (4%)
    reduce_scatter x2, waiting for transfers between devices, sum_by_axis(): so_far = lax.psum_scatter(so_far, axis, scatter_dimension=0, tiled=True)  78.9 us
    all_to_all x1, waiting for transfers between devices, sent_and_summed(): lax.all_to_all(parts, axis, split_axis=0, concat_axis=0, tiled=True)  53.3 us
    all_to_all x2, waiting for transfers between devices, copy_for_each(): return lax.all_to_all(copies, axis, split_axis=0, concat_axis=0, tiled=True)  19.7 us
    dynamic_slice x8, local copies, waits for them, and re-layouts, shards(): score_grads = lax.map(score_grad, (jnp.arange(blocks), stored_scores))  15.3 us
    all_to_all x2, starting transfers between devices, copy_for_each(): return lax.all_to_all(copies, axis, split_axis=0, concat_axis=0, tiled=True)  14.7 us
    dot_general x4, matrix products, gather_stats(): jnp.dot(gathered, weight_block, preferred_element_type=jnp.float32)  14.1 us
    unnamed x18, local copies, waits for them, and re-layouts  13.9 us
    another operation x1, loops' own time, shards(): lax.scan(gather_stats, start_stats, jnp.arange(blocks))  10.6 us
  transfers between devices with their start and end apart: 6, of which 5 were waited for; matrix products, arithmetic and copies ran while one was open for 9% of the time, Pallas kernels for 0%

commit v1 on v0

v1 whole, which is shorter than its diff:
```python
import jax
import jax.numpy as jnp
from jax import lax
from jax.experimental import pallas as pl
from jax.experimental.pallas import tpu as pltpu
from jax.sharding import Mesh
from jax.sharding import PartitionSpec as P

MESH = pl.DeviceIdType.MESH
F32 = jnp.float32
BF16 = jnp.bfloat16
AXES = ("y", "x", "z", "c")

EPSILON = 1e-06
Z_WEIGHT = 0.001
LOSS_SCALE = 32.0

RING = 4
NZ = 8
BLOCK = 32
HALF = 16
CHUNK = 128
ROWS = 512
WIDTH = 2048
COLS = 2048
SUB = 512
NSUB = COLS // SUB
RS_ORDER = (2, 1, 3, 0)
AG_ORDER = (0, 3, 1, 2)


def inverse_rms(values):
    return lax.rsqrt(jnp.mean(values * values, axis=-1, keepdims=True) + EPSILON)


def aligned(start, size, unit):
    return pl.ds(pl.multiple_of(start, unit), size)


def kernel(
    hid, down, res, pg, fg, voc, bias, ids, wts,
    loss_o, sg_o, vg_o,
    hid_v, down_v, res_v, pg_v, fg_v, voc_v, bias_v, ids_v, wts_v,
    part, scores, wanted, normed, grads, stream_v, inv_v,
    ra, rb, rc, sb2, ra2, rb2, rc2, keep2,
    rra, rrb, rrc, rsb2, rra2, rrb2, rrc2,
    lse_c, tgt_c, norm_c, stat_s, stat_r, loss_v,
    v_own, pair_s, pair_r, z_s, z_r, sg_v, vg_v,
    load_sem, hid_sem, out_sem,
    rs_ss, rs_rs, rr_ss, rr_rs, ag_ss, ag_rs, st_ss, st_rs, pr_ss, pr_rs, z_ss, z_rs,
):
    y, x, z, c = (lax.axis_index(name) for name in AXES)
    a = x + c * (y - x)
    b = y + c * (x - y)

    def mod4(value):
        return lax.rem(value, RING)

    def dev_a(step):
        to = mod4(a + step)
        return (y + c * (to - y), to + c * (x - to), z, c)

    def dev_b(step):
        to = mod4(b + step)
        return (to + c * (y - to), x + c * (to - x), z, c)

    up_z = lax.rem(z + 1 + c * (NZ - 2), NZ)
    down_z = lax.rem(z + NZ - 1 - c * (NZ - 2), NZ)
    dev_up = (y, x, up_z, c)
    dev_down = (y, x, down_z, c)
    dev_pair = (y, x, z, 1 - c)

    def source_row(i, q):
        return (i * (1 + 3 * c) + q * (4 - 3 * c)) * BLOCK

    def rows(i, q, h):
        return aligned(i * CHUNK + q * BLOCK + h * HALF, HALF, HALF)

    def rows32(i, q):
        return aligned(i * CHUNK + q * BLOCK, BLOCK, BLOCK)

    def chunk_rows(i):
        return aligned(i * CHUNK, CHUNK, CHUNK)

    def sub_cols(j):
        return aligned(j * SUB, SUB, SUB)

    def remote(src, dst, send, recv, to):
        return pltpu.make_async_remote_copy(
            src_ref=src, dst_ref=dst, send_sem=send, recv_sem=recv,
            device_id=to, device_id_type=MESH,
        )

    a_up, a_dn, a_far = dev_a(1), dev_a(3), dev_a(2)
    b_up, b_dn, b_far = dev_b(1), dev_b(3), dev_b(2)

    barrier = pltpu.get_barrier_semaphore()
    for to in (a_up, a_dn, a_far, b_up, b_dn, b_far, dev_pair, dev_down):
        pl.semaphore_signal(barrier, inc=1, device_id=to, device_id_type=MESH)

    hid_copies = []
    for i in range(RING):
        for q in range(RING):
            hid_copies.append(
                pltpu.make_async_copy(
                    hid.at[aligned(source_row(i, q), BLOCK, BLOCK), :],
                    hid_v.at[pl.ds(i * CHUNK + q * BLOCK, BLOCK), :],
                    hid_sem.at[i * RING + q],
                )
            )
    loads = [
        pltpu.make_async_copy(src, dst, load_sem.at[k])
        for k, (src, dst) in enumerate(
            [
                (down, down_v), (ids, ids_v), (wts, wts_v), (res, res_v),
                (pg, pg_v), (fg, fg_v), (bias, bias_v),
            ]
            + [
                (voc.at[pl.ds(k * SUB, SUB), :], voc_v.at[pl.ds(k * SUB, SUB), :])
                for k in range(WIDTH // SUB)
            ]
        )
    ]
    for copy in hid_copies + loads:
        copy.start()

    def branch_chunk(i, send):
        def piece(n, carry):
            value = jnp.dot(
                hid_v[chunk_rows(i), :], down_v[:, sub_cols(n)], preferred_element_type=F32
            )
            scores[chunk_rows(i), sub_cols(n)] = value
            if send:
                part[chunk_rows(i), sub_cols(n)] = value.astype(BF16)
            return carry

        lax.fori_loop(0, WIDTH // SUB, piece, 0)

    def rs_tools(ra, rb, rc, sb2, ra2, rb2, rc2, ss, rs):
        far, up, dn = mod4(a + 2), mod4(a + 1), mod4(a + 3)

        def q_of(t):
            return mod4(b + RS_ORDER[t])

        def one(kind, t):
            q, k = q_of(t), kind * RING + t
            src, dst, to = (
                (rows(far, q, 0), ra.at[0, t], a_up),
                (rows(far, q, 1), ra.at[1, t], a_dn),
                (rows(up, q, 1), rb.at[0, t], a_up),
                (rows(dn, q, 0), rb.at[1, t], a_dn),
                (rows(up, q, 0), rc.at[0, t], a_up),
                (rows(dn, q, 1), rc.at[1, t], a_dn),
            )[kind]
            return remote(part.at[src, :], dst, ss.at[k], rs.at[k], to)

        def two(kind):
            k = 24 + kind
            src, dst, to = (
                (sb2.at[0, 0], ra2.at[0], b_up),
                (sb2.at[0, 1], ra2.at[1], b_dn),
                (sb2.at[1, 1], rb2.at[0], b_up),
                (sb2.at[2, 0], rb2.at[1], b_dn),
                (sb2.at[1, 0], rc2.at[0], b_up),
                (sb2.at[2, 1], rc2.at[1], b_dn),
            )[kind]
            return remote(src, dst, ss.at[k], rs.at[k], to)

        def first():
            for t in range(RING):
                one(0, t).start()
                one(1, t).start()

        def middle():
            for t in range(RING):
                q = q_of(t)
                one(2, t).start()
                one(3, t).start()
                for kind, i, h in ((0, up, 0), (1, dn, 1)):
                    one(kind, t).wait_recv()
                    part[rows(i, q, h), :] = (
                        scores[rows(i, q, h), :] + ra[h, t].astype(F32)
                    ).astype(BF16)
                    one(4 + kind, t).start()

        def finish_a():
            for t in range(RING):
                q = q_of(t)
                for kind in range(2, 6):
                    one(kind, t).wait_recv()
                low = scores[rows(a, q, 0), :] + rc[0, t].astype(F32) + rb[1, t].astype(F32)
                high = scores[rows(a, q, 1), :] + rb[0, t].astype(F32) + rc[1, t].astype(F32)
                if t == 0:
                    sb2[0, 0] = low.astype(BF16)
                    two(0).start()
                    sb2[0, 1] = high.astype(BF16)
                    two(1).start()
                elif t == 1:
                    sb2[1, 1] = high.astype(BF16)
                    two(2).start()
                    keep2[0] = low
                elif t == 2:
                    sb2[2, 0] = low.astype(BF16)
                    two(3).start()
                    keep2[1] = high
                else:
                    keep2[2] = low
                    keep2[3] = high

        def middle_b():
            two(0).wait_recv()
            sb2[1, 0] = (keep2[0] + ra2[0].astype(F32)).astype(BF16)
            two(4).start()
            two(1).wait_recv()
            sb2[2, 1] = (keep2[1] + ra2[1].astype(F32)).astype(BF16)
            two(5).start()

        def finish_b():
            for kind in range(2, 6):
                two(kind).wait_recv()
            low = keep2[2] + rc2[0].astype(F32) + rb2[1].astype(F32)
            high = keep2[3] + rb2[0].astype(F32) + rc2[1].astype(F32)
            return jnp.concatenate([low, high], axis=0)

        def sent():
            for kind in range(6):
                for t in range(RING):
                    one(kind, t).wait_send()
            for kind in range(6):
                two(kind).wait_send()

        return first, middle, finish_a, middle_b, finish_b, sent

    def wanted_block(p):
        i, q = p // RING, lax.rem(p, RING)
        at = aligned(source_row(i, q), BLOCK, BLOCK)
        local = ids_v[at, :] - (y * RING + x) * COLS
        weight = wts_v[at, :]
        for n in range(NSUB):
            position = lax.broadcasted_iota(jnp.int32, (BLOCK, SUB), 1) + n * SUB
            total = jnp.zeros((BLOCK, SUB), F32)
            for k in range(4):
                total = total + jnp.where(
                    local[:, k : k + 1] == position, weight[:, k : k + 1], 0.0
                )
            wanted[aligned(p * BLOCK, BLOCK, BLOCK), pl.ds(n * SUB, SUB)] = total

    def wanted_blocks(start, stop):
        def body(p, carry):
            wanted_block(p)
            return carry

        lax.fori_loop(start, stop, body, 0)

    first, middle, finish_a, middle_b, finish_b, sent = rs_tools(
        ra, rb, rc, sb2, ra2, rb2, rc2, rs_ss, rs_rs
    )
    for copy in hid_copies:
        copy.wait()
    loads[0].wait()
    branch_chunk(mod4(a + 2), True)
    pl.semaphore_wait(barrier, 8)
    first()
    branch_chunk(mod4(a + 1), True)
    branch_chunk(mod4(a + 3), True)
    branch_chunk(a, False)
    for copy in loads[1:7]:
        copy.wait()
    wanted_blocks(0, 8)
    middle()
    wanted_blocks(8, 16)
    finish_a()
    middle_b()
    branch = finish_b()

    stream = res_v[...].astype(F32) + branch * inverse_rms(branch) * pg_v[...]
    inverse = inverse_rms(stream)
    stream_v[...] = stream
    inv_v[...] = jnp.broadcast_to(inverse, inv_v.shape)
    normed[rows32(a, b), :] = (stream * inverse * fg_v[...]).astype(BF16)

    up, dn, far = mod4(a + 1), mod4(a + 3), mod4(a + 2)
    b1, b3, b2 = mod4(b + 1), mod4(b + 3), mod4(b + 2)

    def gather_b(kind, arriving=False):
        at, to = (
            (rows32(a, b3 if arriving else b), b_up),
            (rows32(a, b1 if arriving else b), b_dn),
            (rows(a, b2 if arriving else b3, 0), b_up),
            (rows(a, b2 if arriving else b1, 1), b_dn),
        )[kind]
        return remote(normed.at[at, :], normed.at[at, :], ag_ss.at[kind], ag_rs.at[kind], to)

    def gather_a(kind, t, arriving=False):
        q = mod4(b + AG_ORDER[t])
        at, to = (
            (rows32(dn if arriving else a, q), a_up),
            (rows32(up if arriving else a, q), a_dn),
            (rows(far if arriving else dn, q, 0), a_up),
            (rows(far if arriving else up, q, 1), a_dn),
        )[kind]
        k = 4 + t * 4 + kind
        return remote(normed.at[at, :], normed.at[at, :], ag_ss.at[k], ag_rs.at[k], to)

    def forward_a(t):
        for kind in (0, 1):
            gather_a(kind, t, True).wait_recv()
            gather_a(2 + kind, t).start()

    for kind in (0, 1):
        gather_b(kind).start()
        gather_a(kind, 0).start()
    for kind in (0, 1):
        gather_b(kind, True).wait_recv()
        gather_b(2 + kind).start()
        gather_a(0, 1 + kind).start()
        gather_a(1, 1 + kind).start()
    forward_a(0)
    for kind in (2, 3):
        gather_b(kind, True).wait_recv()
    for kind in (0, 1):
        gather_a(kind, 3).start()
    for copy in loads[7:]:
        copy.wait()

    def score_pieces(i, start, stop):
        def piece(n, carry):
            value = jnp.dot(
                normed[chunk_rows(i), :], voc_v[:, sub_cols(n)], preferred_element_type=F32
            )
            scores[chunk_rows(i), sub_cols(n)] = value + bias_v[:, sub_cols(n)]
            return carry

        lax.fori_loop(start, stop, piece, 0)

    def stats(i):
        def body(r, carry):
            at = aligned(i * CHUNK + r * HALF, HALF, HALF)
            value = scores[at, :]
            peak = jnp.max(value, axis=1, keepdims=True)
            total = jnp.sum(jnp.exp(value - peak), axis=1, keepdims=True)
            target = jnp.sum(wanted[at, :] * value, axis=1, keepdims=True)
            lse_c[at, :] = jnp.broadcast_to(peak + jnp.log(total), (HALF, 128))
            tgt_c[at, :] = jnp.broadcast_to(target, (HALF, 128))
            return carry

        lax.fori_loop(0, CHUNK // HALF, body, 0)
        stat_s[0, pl.ds(i, 1), :] = jnp.transpose(lse_c[chunk_rows(i), :])[0:1, :]
        stat_s[0, pl.ds(i + RING, 1), :] = jnp.transpose(tgt_c[chunk_rows(i), :])[0:1, :]

    score_pieces(a, 0, 2)
    forward_a(1)
    score_pieces(a, 2, 4)
    forward_a(2)
    stats(a)
    forward_a(3)
    for i in (up, dn):
        score_pieces(i, 0, 4)
        stats(i)
    for t in range(RING):
        for kind in (2, 3):
            gather_a(kind, t, True).wait_recv()
    score_pieces(far, 0, 4)
    stats(far)

    def stat_copy(phase, k):
        to = ((a_up, a_dn, a_far), (b_up, b_dn, b_far))[phase][k]
        n = phase * 3 + k
        return remote(stat_s.at[phase], stat_r.at[n], st_ss.at[n], st_rs.at[n], to)

    is_lse = lax.broadcasted_iota(jnp.int32, (8, 128), 0) < RING
    for phase in range(2):
        for k in range(3):
            stat_copy(phase, k).start()
        for k in range(3):
            stat_copy(phase, k).wait_recv()
        parts = [stat_s[phase]] + [stat_r[phase * 3 + k] for k in range(3)]
        peak = jnp.maximum(jnp.maximum(parts[0], parts[1]), jnp.maximum(parts[2], parts[3]))
        joint = peak + jnp.log(sum(jnp.exp(value - peak) for value in parts))
        stat_s[phase + 1] = jnp.where(is_lse, joint, sum(parts))
    log_rows = stat_s[2, 0:RING, :]
    for i in range(RING):
        norm_c[pl.ds(i * CHUNK, CHUNK), :] = jnp.transpose(
            jnp.broadcast_to(stat_s[2, i : i + 1, :], (CHUNK, 128))
        )
    loss_v[...] = log_rows - stat_s[2, RING:8, :] + Z_WEIGHT * log_rows * log_rows

    def grad_block(j):
        def body(r, carry):
            at = aligned(r * BLOCK, BLOCK, BLOCK)
            log_norm = norm_c[at, :]
            factor = 1.0 + 2.0 * Z_WEIGHT * log_norm
            for n in range(SUB // 128):
                cols = aligned(j * SUB + n * 128, 128, 128)
                probability = jnp.exp(scores[at, cols] - log_norm)
                grads[at, cols] = (
                    LOSS_SCALE * (probability * factor - wanted[at, cols])
                ).astype(BF16)
            return carry

        lax.fori_loop(0, ROWS // BLOCK, body, 0)

    def pair_copy(s, j):
        k = s * NSUB + j
        return remote(pair_s.at[k], pair_r.at[k], pr_ss.at[k], pr_rs.at[k], dev_pair)

    def z_copy(s, j):
        k = s * NSUB + j
        return remote(z_s.at[k], z_r.at[k], z_ss.at[k], z_rs.at[k], dev_up)

    def vocab_piece(s, j):
        away = (1 - 2 * c) * (1 + s)
        own_dest = lax.rem(z + 2 * NZ - away, NZ) * 2 + c
        pair_dest = lax.rem(z + 2 * NZ + away, NZ) * 2 + 1 - c
        both = jnp.concatenate(
            [normed[:, aligned(dest * CHUNK, CHUNK, CHUNK)] for dest in (own_dest, pair_dest)], axis=1
        )
        value = lax.dot_general(
            both, grads[:, sub_cols(j)], (((0,), (0,)), ((), ())), preferred_element_type=F32
        )
        v_own[(s % 2) * NSUB + j] = value[0:CHUNK]
        pair_s[s * NSUB + j] = value[CHUNK:].astype(BF16)
        pair_copy(s, j).start()

    def z_piece(s, j):
        k = s * NSUB + j
        pair_copy(s, j).wait_recv()
        value = v_own[(s % 2) * NSUB + j] + pair_r[k].astype(F32)
        if s > 0:
            z_copy(s - 1, j).wait_recv()
            value = value + z_r[k - NSUB].astype(F32)
        if s < NZ - 1:
            z_s[k] = value.astype(BF16)
            z_copy(s, j).start()
        else:
            vg_v[j] = value
            out_copy(j).start()

    def out_copy(j):
        return pltpu.make_async_copy(vg_v.at[j], vg_o.at[:, sub_cols(j)], out_sem.at[j])

    def row_piece(i, n):
        value = lax.dot_general(
            grads[chunk_rows(i), :], voc_v[sub_cols(n), :],
            (((1,), (1,)), ((), ())), preferred_element_type=F32,
        )
        scores[chunk_rows(i), sub_cols(n)] = value
        part[chunk_rows(i), sub_cols(n)] = value.astype(BF16)

    for j in range(NSUB):
        grad_block(j)
        vocab_piece(0, j)
        if j > 0:
            z_piece(0, j - 1)
    z_piece(0, NSUB - 1)
    sent()

    first, middle, finish_a, middle_b, finish_b, sent_rows = rs_tools(
        rra, rrb, rrc, rsb2, rra2, rrb2, rrc2, rr_ss, rr_rs
    )
    row_order = (far, up, dn, a)
    for s in range(NZ):

        def slot(j, carry):
            if s > 0:
                z_piece(s, j)
            if s < NZ - 1:
                vocab_piece(s + 1, j)
            if s < RING:
                row_piece(row_order[s], j)
            return carry

        lax.fori_loop(0, NSUB, slot, 0)
        if s == 0:
            first()
        elif s == 2:
            middle()
        elif s == 4:
            finish_a()
        elif s == 5:
            middle_b()
        elif s == 6:
            stream = stream_v[...]
            inverse = inv_v[:, 0:1]
            upstream = finish_b() * fg_v[...]
            sg_v[...] = inverse * (
                upstream
                - stream * inverse * inverse * jnp.mean(upstream * stream, axis=-1, keepdims=True)
            )
            pltpu.make_async_copy(sg_v, sg_o, out_sem.at[NSUB]).start()
            own = jnp.broadcast_to(loss_v[pl.ds(a, 1), :], (8, 128))
            own = pltpu.roll(own, lax.rem(128 - b * BLOCK, 128), 1)
            loss_o[...] = own[0:1, 0:BLOCK]

    sent_rows()
    for kind in range(4):
        gather_b(kind).wait_send()
        for t in range(RING):
            gather_a(kind, t).wait_send()
    for phase in range(2):
        for k in range(3):
            stat_copy(phase, k).wait_send()

    def drain_pair(k, carry):
        pair_copy(0, k).wait_send()
        return carry

    def drain_z(k, carry):
        z_copy(0, k).wait_send()
        return carry

    lax.fori_loop(0, NZ * NSUB, drain_pair, 0)
    lax.fori_loop(0, (NZ - 1) * NSUB, drain_z, 0)
    for j in range(NSUB):
        out_copy(j).wait()
    pltpu.make_async_copy(sg_v, sg_o, out_sem.at[NSUB]).wait()


def shards(hid, down, res, pg, fg, voc, bias, ids, wts):
    hbm = pl.BlockSpec(memory_space=pl.ANY)
    vmem = pltpu.VMEM
    dma = pltpu.SemaphoreType.DMA
    rs_bufs = [
        vmem((2, RING, HALF, WIDTH), BF16),
        vmem((2, RING, HALF, WIDTH), BF16),
        vmem((2, RING, HALF, WIDTH), BF16),
        vmem((3, 2, HALF, WIDTH), BF16),
        vmem((2, HALF, WIDTH), BF16),
        vmem((2, HALF, WIDTH), BF16),
        vmem((2, HALF, WIDTH), BF16),
    ]
    scratch = [
        vmem((ROWS, 512), BF16),
        vmem((512, WIDTH), BF16),
        vmem((BLOCK, WIDTH), BF16),
        vmem((1, WIDTH), F32),
        vmem((1, WIDTH), F32),
        vmem((WIDTH, COLS), BF16),
        vmem((1, COLS), F32),
        vmem((ROWS, 4), jnp.int32),
        vmem((ROWS, 4), F32),
        vmem((ROWS, WIDTH), BF16),
        vmem((ROWS, COLS), F32),
        vmem((ROWS, COLS), F32),
        vmem((ROWS, WIDTH), BF16),
        vmem((ROWS, COLS), BF16),
        vmem((BLOCK, WIDTH), F32),
        vmem((BLOCK, 128), F32),
        *rs_bufs,
        vmem((4, HALF, WIDTH), F32),
        *rs_bufs,
        vmem((ROWS, 128), F32),
        vmem((ROWS, 128), F32),
        vmem((ROWS, 128), F32),
        vmem((3, 8, 128), F32),
        vmem((6, 8, 128), F32),
        vmem((RING, 128), F32),
        vmem((2 * NSUB, CHUNK, SUB), F32),
        vmem((NZ * NSUB, CHUNK, SUB), BF16),
        vmem((NZ * NSUB, CHUNK, SUB), BF16),
        vmem(((NZ - 1) * NSUB, CHUNK, SUB), BF16),
        vmem(((NZ - 1) * NSUB, CHUNK, SUB), BF16),
        vmem((BLOCK, WIDTH), F32),
        vmem((NSUB, CHUNK, SUB), F32),
        dma((11,)),
        dma((16,)),
        dma((NSUB + 1,)),
        *[dma((30,))] * 4,
        *[dma((20,))] * 2,
        *[dma((6,))] * 2,
        *[dma((NZ * NSUB,))] * 2,
        *[dma(((NZ - 1) * NSUB,))] * 2,
    ]
    losses, stream_grad, vocab_grad = pl.pallas_call(
        kernel,
        out_shape=(
            jax.ShapeDtypeStruct((1, BLOCK), F32),
            jax.ShapeDtypeStruct((BLOCK, WIDTH), F32),
            jax.ShapeDtypeStruct((CHUNK, COLS), F32),
        ),
        in_specs=[hbm] * 9,
        out_specs=(pl.BlockSpec(memory_space=pltpu.VMEM), pl.BlockSpec(memory_space=pltpu.HBM), pl.BlockSpec(memory_space=pltpu.HBM)),
        scratch_shapes=scratch,
        compiler_params=pltpu.CompilerParams(
            collective_id=0, has_side_effects=True, vmem_limit_bytes=60 * 1024 * 1024
        ),
    )(hid, down, res, pg.reshape(1, WIDTH), fg.reshape(1, WIDTH), voc,
      bias.reshape(1, COLS), ids, wts)
    return losses.reshape(BLOCK), stream_grad, vocab_grad


def solution(mesh):
    split = Mesh(mesh.devices.reshape(4, 4, 8, 2), AXES)
    vp, dp = ("y", "x"), ("z", "c")
    return jax.shard_map(
        shards,
        mesh=split,
        in_specs=(
            P(dp, vp),
            P(vp, None),
            P(dp + vp, None),
            P(),
            P(),
            P(None, vp),
            P(vp),
            P(dp, None),
            P(dp, None),
        ),
        out_specs=(P(dp + vp), P(dp + vp, None), P(dp, vp)),
        check_vma=False,
    )
```

time: 309 us -> 121 us (0.39); the launches traced: 303 us -> 121 us
  waiting for transfers between devices: 152 us -> 0 us
  Pallas kernels: 0 us -> 112 us
  matrix products: 38.8 us -> 0 us
  local copies, waits for them, and re-layouts: 45.8 us -> 8.18 us
  starting transfers between devices: 20.7 us -> 0 us
  other arithmetic: 18.4 us -> 0 us
  between operations: 14 us -> 0.64 us
  loops' own time: 13.3 us -> 0 us
    pallas_call x0 -> x1, Pallas kernels: none -> 112 us  [shards(): pl.pallas_call(kernel, out_shape=(jax.ShapeDtypeStruct((1, BLOCK), F32),...]
    reduce_scatter x3 -> x0, waiting for transfers between devices: 78.9 us -> none  [the longest x2 78.9 us: sum_by_axis(): so_far = lax.psum_scatter(so_far, axis, scatter_dimension=0, tiled=True)]
    all_to_all x3 -> x0, waiting for transfers between devices: 73 us -> none  [the longest x1 53.3 us: sent_and_summed(): lax.all_to_all(parts, axis, split_axis=0, concat_axis=0, tiled=True)]
    dot_general x7 -> x0, matrix products: 38.8 us -> none  [the longest x4 14.1 us: gather_stats(): jnp.dot(gathered, weight_block, preferred_element_type=jnp.float32)]
    dynamic_slice x21 -> x0, local copies, waits for them, and re-layouts: 20.6 us -> none  [the longest x8 15.3 us: shards(): score_grads = lax.map(score_grad, (jnp.arange(blocks), stored_scores))]
    all_to_all x3 -> x0, starting transfers between devices: 20.4 us -> none  [the longest x2 14.7 us: copy_for_each(): return lax.all_to_all(copies, axis, split_axis=0, concat_axis=0, tiled=True)]
    another operation x2 -> x0, loops' own time: 13.3 us -> none  [the longest x1 10.6 us: shards(): lax.scan(gather_stats, start_stats, jnp.arange(blocks))]
    reduce_sum x8 -> x0, other arithmetic: 7.57 us -> none  [the longest x4 2.6 us: gather_stats(): run_target = run_target + jnp.sum(wanted * scores, axis=1)]
  transfers between devices with their start and end apart: 6 -> 0, of which waited for: 5 -> 0; matrix products, arithmetic and copies ran while one was open for 9% -> 0% of each run, Pallas kernels for 0% -> 0%
where the time goes in v1:
time: 121 us
  Pallas kernels  112 us (93%)
  local copies, waits for them, and re-layouts  8.18 us (7%)
    pallas_call x1, Pallas kernels, shards(): pl.pallas_call(kernel, out_shape=(jax.ShapeDtypeStruct((1, BLOCK), F32),...  112 us
    unnamed x5, local copies, waits for them, and re-layouts  8.18 us

profile of v1, /device:TPU:2, one launch (start us, length us, event | category | flops | bytes accessed | tf_op | source)
XLA Modules:
  0.0 120.6 jit_solution(11462736849605571431)
XLA Ops:
  0.6 1.6 %copy.12.ids = s32[512,4]{1,0:T(8,128)} copy(s32[512,4]{0,1:T(4,128)} %param.16) | data formatting | bytes 16384 | tf_op args[7]
  2.2 1.5 %copy.13.wts = f32[512,4]{1,0:T(8,128)} copy(f32[512,4]{0,1:T(4,128)} %param.17) | data formatting | bytes 16384 | tf_op args[8]
  3.7 111.8 %shard_map.112 = (f32[1,32]{1,0:T(1,128)}, f32[32,2048]{1,0:T(8,128)}, f32[128,2048]{1,0:T(8,128)}) custom-call(bf16[512,512]{1,0:T(8,128)(2,1)} %hid.1, bf16[512,2048]{1,0:T(8,128)(2,1)} %down.1, bf16[32,2048]{1,0:T(8,128)(2,1)} %res.1, f32[1,2048]{1,0:T(1,128)} %bitcast.4, f32[1,2048]{1,0:T(1,128)} %bitcast.5, bf16[2048,2048]{1,0:T(8,128)(2,1)} %voc.1, ...), custom_call_target="tpu_custom_call" | custom-call | tf_op jit(solution)/shard_map/pallas_call | solution.py:574
  115.5 1.1 copy.17
  116.7 1.7 %copy.18 = f32[32,2048]{1,0:T(8,128)} copy(f32[32,2048]{1,0:T(8,128)} %get-tuple-element.13) | data formatting | bytes 524288
  118.3 2.3 %copy.19 = f32[128,2048]{1,0:T(8,128)} copy(f32[128,2048]{1,0:T(8,128)} %get-tuple-element.14) | data formatting | bytes 2097152

commit v2 on v1

--- a/solution.py
+++ b/solution.py
@@ -40,11 +40,11 @@
 def kernel(
     hid, down, res, pg, fg, voc, bias, ids, wts,
     loss_o, sg_o, vg_o,
-    hid_v, down_v, res_v, pg_v, fg_v, voc_v, bias_v, ids_v, wts_v,
+    hid_v, down_v, res_v, pg_v, fg_v, voc_v, bias_v, ids_v, wts_v, meta_v,
     part, scores, wanted, normed, grads, stream_v, inv_v,
     ra, rb, rc, sb2, ra2, rb2, rc2, keep2,
     rra, rrb, rrc, rsb2, rra2, rrb2, rrc2,
-    lse_c, tgt_c, norm_c, stat_s, stat_r, loss_v,
+    stat_c, turn_v, norm_c, stat_s, stat_r, loss_v, loss_out,
     v_own, pair_s, pair_r, z_s, z_r, sg_v, vg_v,
     load_sem, hid_sem, out_sem,
     rs_ss, rs_rs, rr_ss, rr_rs, ag_ss, ag_rs, st_ss, st_rs, pr_ss, pr_rs, z_ss, z_rs,
@@ -91,6 +91,12 @@
             device_id=to, device_id_type=MESH,
         )
 
+    def arrived(view, sem):
+        remote(view, view, sem, sem, dev_pair).wait_recv()
+
+    def gone(view, sem):
+        remote(view, view, sem, sem, dev_pair).wait_send()
+
     a_up, a_dn, a_far = dev_a(1), dev_a(3), dev_a(2)
     b_up, b_dn, b_far = dev_b(1), dev_b(3), dev_b(2)
 
@@ -105,26 +111,24 @@
                 pltpu.make_async_copy(
                     hid.at[aligned(source_row(i, q), BLOCK, BLOCK), :],
                     hid_v.at[pl.ds(i * CHUNK + q * BLOCK, BLOCK), :],
-                    hid_sem.at[i * RING + q],
+                    hid_sem,
                 )
             )
+    pairs = [(down.at[:, pl.ds(k * SUB, SUB)], down_v.at[:, pl.ds(k * SUB, SUB)]) for k in range(4)]
+    pairs += [
+        (ids, ids_v), (wts, wts_v), (res, res_v), (pg, pg_v), (fg, fg_v), (bias, bias_v),
+    ]
+    pairs += [
+        (voc.at[pl.ds(k * SUB, SUB), :], voc_v.at[pl.ds(k * SUB, SUB), :]) for k in range(4)
+    ]
     loads = [
-        pltpu.make_async_copy(src, dst, load_sem.at[k])
-        for k, (src, dst) in enumerate(
-            [
-                (down, down_v), (ids, ids_v), (wts, wts_v), (res, res_v),
-                (pg, pg_v), (fg, fg_v), (bias, bias_v),
-            ]
-            + [
-                (voc.at[pl.ds(k * SUB, SUB), :], voc_v.at[pl.ds(k * SUB, SUB), :])
-                for k in range(WIDTH // SUB)
-            ]
-        )
+        pltpu.make_async_copy(src, dst, load_sem.at[min(k, 10)])
+        for k, (src, dst) in enumerate(pairs)
     ]
-    for copy in hid_copies + loads:
+    for copy in hid_copies + loads[0:4]:
         copy.start()
 
-    def branch_chunk(i, send):
+    def branch_chunk(i, send, ready=None):
         def piece(n, carry):
             value = jnp.dot(
                 hid_v[chunk_rows(i), :], down_v[:, sub_cols(n)], preferred_element_type=F32
@@ -134,7 +138,12 @@
                 part[chunk_rows(i), sub_cols(n)] = value.astype(BF16)
             return carry
 
-        lax.fori_loop(0, WIDTH // SUB, piece, 0)
+        if ready is None:
+            lax.fori_loop(0, WIDTH // SUB, piece, 0)
+        else:
+            for n in range(WIDTH // SUB):
+                ready[n].wait()
+                piece(n, 0)
 
     def rs_tools(ra, rb, rc, sb2, ra2, rb2, rc2, ss, rs):
         far, up, dn = mod4(a + 2), mod4(a + 1), mod4(a + 3)
@@ -143,7 +152,7 @@
             return mod4(b + RS_ORDER[t])
 
         def one(kind, t):
-            q, k = q_of(t), kind * RING + t
+            q = q_of(t)
             src, dst, to = (
                 (rows(far, q, 0), ra.at[0, t], a_up),
                 (rows(far, q, 1), ra.at[1, t], a_dn),
@@ -152,10 +161,10 @@
                 (rows(up, q, 0), rc.at[0, t], a_up),
                 (rows(dn, q, 1), rc.at[1, t], a_dn),
             )[kind]
-            return remote(part.at[src, :], dst, ss.at[k], rs.at[k], to)
+            recv = rs.at[t if kind < 2 else RING + t]
+            return remote(part.at[src, :], dst, ss, recv, to)
 
         def two(kind):
-            k = 24 + kind
             src, dst, to = (
                 (sb2.at[0, 0], ra2.at[0], b_up),
                 (sb2.at[0, 1], ra2.at[1], b_dn),
@@ -164,30 +173,33 @@
                 (sb2.at[1, 0], rc2.at[0], b_up),
                 (sb2.at[2, 1], rc2.at[1], b_dn),
             )[kind]
-            return remote(src, dst, ss.at[k], rs.at[k], to)
+            return remote(src, dst, ss, rs.at[8 + min(kind, 2)], to)
 
         def first():
             for t in range(RING):
                 one(0, t).start()
                 one(1, t).start()
 
+        def second(t):
+            one(2, t).start()
+            one(3, t).start()
+
         def middle():
             for t in range(RING):
                 q = q_of(t)
-                one(2, t).start()
-                one(3, t).start()
+                arrived(ra.at[:, t], rs.at[t])
                 for kind, i, h in ((0, up, 0), (1, dn, 1)):
-                    one(kind, t).wait_recv()
                     part[rows(i, q, h), :] = (
                         scores[rows(i, q, h), :] + ra[h, t].astype(F32)
                     ).astype(BF16)
                     one(4 + kind, t).start()
-
-        def finish_a():
-            for t in range(RING):
+                if t < 2:
+                    second(t + 2)
+
+        def finish_a(turns):
+            for t in turns:
                 q = q_of(t)
-                for kind in range(2, 6):
-                    one(kind, t).wait_recv()
+                arrived(part.at[pl.ds(0, 4 * HALF), :], rs.at[RING + t])
                 low = scores[rows(a, q, 0), :] + rc[0, t].astype(F32) + rb[1, t].astype(F32)
                 high = scores[rows(a, q, 1), :] + rb[0, t].astype(F32) + rc[1, t].astype(F32)
                 if t == 0:
@@ -216,28 +228,23 @@
             two(5).start()
 
         def finish_b():
-            for kind in range(2, 6):
-                two(kind).wait_recv()
+            arrived(part.at[pl.ds(0, 4 * HALF), :], rs.at[10])
             low = keep2[2] + rc2[0].astype(F32) + rb2[1].astype(F32)
             high = keep2[3] + rb2[0].astype(F32) + rc2[1].astype(F32)
             return jnp.concatenate([low, high], axis=0)
 
         def sent():
-            for kind in range(6):
-                for t in range(RING):
-                    one(kind, t).wait_send()
-            for kind in range(6):
-                two(kind).wait_send()
-
-        return first, middle, finish_a, middle_b, finish_b, sent
+            gone(part.at[pl.ds(0, 30 * HALF), :], ss)
+
+        return first, second, middle, finish_a, middle_b, finish_b, sent
 
     def wanted_block(p):
         i, q = p // RING, lax.rem(p, RING)
         at = aligned(source_row(i, q), BLOCK, BLOCK)
-        local = ids_v[at, :] - (y * RING + x) * COLS
-        weight = wts_v[at, :]
+        local = meta_v[at, 0:4] - ((y * RING + x) * COLS).astype(F32)
+        weight = meta_v[at, 4:8]
         for n in range(NSUB):
-            position = lax.broadcasted_iota(jnp.int32, (BLOCK, SUB), 1) + n * SUB
+            position = (lax.broadcasted_iota(jnp.int32, (BLOCK, SUB), 1) + n * SUB).astype(F32)
             total = jnp.zeros((BLOCK, SUB), F32)
             for k in range(4):
                 total = total + jnp.where(
@@ -252,25 +259,33 @@
 
         lax.fori_loop(start, stop, body, 0)
 
-    first, middle, finish_a, middle_b, finish_b, sent = rs_tools(
+    first, second, middle, finish_a, middle_b, finish_b, sent = rs_tools(
         ra, rb, rc, sb2, ra2, rb2, rc2, rs_ss, rs_rs
     )
-    for copy in hid_copies:
-        copy.wait()
-    loads[0].wait()
-    branch_chunk(mod4(a + 2), True)
+    pltpu.make_async_copy(hid, hid_v, hid_sem).wait()
+    branch_chunk(mod4(a + 2), True, loads[0:4])
+    for copy in loads[4:]:
+        copy.start()
     pl.semaphore_wait(barrier, 8)
     first()
     branch_chunk(mod4(a + 1), True)
     branch_chunk(mod4(a + 3), True)
+    second(0)
+    second(1)
     branch_chunk(a, False)
-    for copy in loads[1:7]:
+    middle()
+    for copy in loads[4:10]:
         copy.wait()
+    for g in range(RING):
+        lanes = pl.ds(g * 128, 128)
+        both = jnp.concatenate([ids_v[:, lanes].astype(F32), wts_v[:, lanes]], axis=0)
+        meta_v[lanes, :] = jnp.transpose(jnp.concatenate([both] * 16, axis=0))
     wanted_blocks(0, 8)
-    middle()
+    finish_a((0,))
     wanted_blocks(8, 16)
-    finish_a()
+    finish_a((1, 2))
     middle_b()
+    finish_a((3,))
     branch = finish_b()
 
     stream = res_v[...].astype(F32) + branch * inverse_rms(branch) * pg_v[...]
@@ -289,7 +304,9 @@
             (rows(a, b2 if arriving else b3, 0), b_up),
             (rows(a, b2 if arriving else b1, 1), b_dn),
         )[kind]
-        return remote(normed.at[at, :], normed.at[at, :], ag_ss.at[kind], ag_rs.at[kind], to)
+        return remote(
+            normed.at[at, :], normed.at[at, :], ag_ss.at[kind // 2], ag_rs.at[min(kind, 2)], to
+        )
 
     def gather_a(kind, t, arriving=False):
         q = mod4(b + AG_ORDER[t])
@@ -299,8 +316,8 @@
             (rows(far if arriving else dn, q, 0), a_up),
             (rows(far if arriving else up, q, 1), a_dn),
         )[kind]
-        k = 4 + t * 4 + kind
-        return remote(normed.at[at, :], normed.at[at, :], ag_ss.at[k], ag_rs.at[k], to)
+        recv = ag_rs.at[3 + 2 * t + kind if kind < 2 else 11]
+        return remote(normed.at[at, :], normed.at[at, :], ag_ss.at[1], recv, to)
 
     def forward_a(t):
         for kind in (0, 1):
@@ -309,71 +326,90 @@
 
     for kind in (0, 1):
         gather_b(kind).start()
+    gone(normed.at[pl.ds(0, 2 * BLOCK), :], ag_ss.at[0])
+    for kind in (0, 1):
         gather_a(kind, 0).start()
     for kind in (0, 1):
         gather_b(kind, True).wait_recv()
         gather_b(2 + kind).start()
+    for kind in (0, 1):
         gather_a(0, 1 + kind).start()
         gather_a(1, 1 + kind).start()
     forward_a(0)
-    for kind in (2, 3):
-        gather_b(kind, True).wait_recv()
+    arrived(normed.at[rows32(a, b2), :], ag_rs.at[2])
     for kind in (0, 1):
         gather_a(kind, 3).start()
-    for copy in loads[7:]:
-        copy.wait()
-
-    def score_pieces(i, start, stop):
+    pltpu.make_async_copy(voc, voc_v, load_sem.at[10]).wait()
+
+    def score_pieces(chunks, start, stop):
         def piece(n, carry):
+            rows_in = [normed[chunk_rows(i), :] for i in chunks]
             value = jnp.dot(
-                normed[chunk_rows(i), :], voc_v[:, sub_cols(n)], preferred_element_type=F32
+                jnp.concatenate(rows_in, axis=0), voc_v[:, sub_cols(n)], preferred_element_type=F32
+            ) + bias_v[:, sub_cols(n)]
+            for k, i in enumerate(chunks):
+                scores[chunk_rows(i), sub_cols(n)] = value[k * CHUNK : (k + 1) * CHUNK]
+            return carry
+
+        lax.fori_loop(start, stop, piece, 0)
+
+    first_lane = lax.broadcasted_iota(jnp.int32, (64, 128), 1) == 0
+
+    def stats(i):
+        for r in range(2):
+            at = aligned(i * CHUNK + r * 64, 64, 64)
+            groups = [pl.ds(g * 128, 128) for g in range(COLS // 128)]
+            peak = scores[at, groups[0]]
+            for group in groups[1:]:
+                peak = jnp.maximum(peak, scores[at, group])
+            peak = jnp.broadcast_to(jnp.max(peak, axis=1, keepdims=True), (64, 128))
+            total = jnp.zeros((64, 128), F32)
+            target = jnp.zeros((64, 128), F32)
+            for group in groups:
+                value = scores[at, group]
+                total = total + jnp.exp(value - peak)
+                target = target + wanted[at, group] * value
+            lse = peak + jnp.log(jnp.sum(total, axis=1, keepdims=True))
+            stat_c[pl.ds(r * 64, 64), :] = jnp.where(
+                first_lane, lse, jnp.sum(target, axis=1, keepdims=True)
             )
-            scores[chunk_rows(i), sub_cols(n)] = value + bias_v[:, sub_cols(n)]
-            return carry
-
-        lax.fori_loop(start, stop, piece, 0)
-
-    def stats(i):
-        def body(r, carry):
-            at = aligned(i * CHUNK + r * HALF, HALF, HALF)
-            value = scores[at, :]
-            peak = jnp.max(value, axis=1, keepdims=True)
-            total = jnp.sum(jnp.exp(value - peak), axis=1, keepdims=True)
-            target = jnp.sum(wanted[at, :] * value, axis=1, keepdims=True)
-            lse_c[at, :] = jnp.broadcast_to(peak + jnp.log(total), (HALF, 128))
-            tgt_c[at, :] = jnp.broadcast_to(target, (HALF, 128))
-            return carry
-
-        lax.fori_loop(0, CHUNK // HALF, body, 0)
-        stat_s[0, pl.ds(i, 1), :] = jnp.transpose(lse_c[chunk_rows(i), :])[0:1, :]
-        stat_s[0, pl.ds(i + RING, 1), :] = jnp.transpose(tgt_c[chunk_rows(i), :])[0:1, :]
-
-    score_pieces(a, 0, 2)
+        turned = jnp.transpose(stat_c[...])
+        stat_s[0, pl.ds(i, 1), :] = turned[0:1, :]
+        stat_s[0, pl.ds(i + RING, 1), :] = turned[1:2, :]
+
+    score_pieces((a,), 0, 2)
     forward_a(1)
-    score_pieces(a, 2, 4)
+    score_pieces((a,), 2, 4)
     forward_a(2)
     stats(a)
     forward_a(3)
-    for i in (up, dn):
-        score_pieces(i, 0, 4)
-        stats(i)
-    for t in range(RING):
-        for kind in (2, 3):
-            gather_a(kind, t, True).wait_recv()
-    score_pieces(far, 0, 4)
+    score_pieces((up, dn), 0, 4)
+    stats(up)
+    stats(dn)
+    arrived(normed.at[chunk_rows(far), :], ag_rs.at[11])
+    score_pieces((far,), 0, 4)
     stats(far)
 
     def stat_copy(phase, k):
         to = ((a_up, a_dn, a_far), (b_up, b_dn, b_far))[phase][k]
         n = phase * 3 + k
-        return remote(stat_s.at[phase], stat_r.at[n], st_ss.at[n], st_rs.at[n], to)
+        return remote(stat_s.at[phase], stat_r.at[n], st_ss, st_rs.at[phase], to)
+
+    def vocab_rows(s):
+        away = (1 - 2 * c) * (1 + s)
+        own_dest = lax.rem(z + 2 * NZ - away, NZ) * 2 + c
+        pair_dest = lax.rem(z + 2 * NZ + away, NZ) * 2 + 1 - c
+        return jnp.concatenate(
+            [normed[:, aligned(dest * CHUNK, CHUNK, CHUNK)] for dest in (own_dest, pair_dest)], axis=1
+        )
 
     is_lse = lax.broadcasted_iota(jnp.int32, (8, 128), 0) < RING
     for phase in range(2):
         for k in range(3):
             stat_copy(phase, k).start()
-        for k in range(3):
-            stat_copy(phase, k).wait_recv()
+        if phase == 0:
+            turn_v[...] = jnp.transpose(vocab_rows(0))
+        arrived(stat_r.at[pl.ds(phase * 3, 3)], st_rs.at[phase])
         parts = [stat_s[phase]] + [stat_r[phase * 3 + k] for k in range(3)]
         peak = jnp.maximum(jnp.maximum(parts[0], parts[1]), jnp.maximum(parts[2], parts[3]))
         joint = peak + jnp.log(sum(jnp.exp(value - peak) for value in parts))
@@ -387,7 +423,7 @@
 
     def grad_block(j):
         def body(r, carry):
-            at = aligned(r * BLOCK, BLOCK, BLOCK)
+            at = aligned(r * 64, 64, 64)
             log_norm = norm_c[at, :]
             factor = 1.0 + 2.0 * Z_WEIGHT * log_norm
             for n in range(SUB // 128):
@@ -398,26 +434,24 @@
                 ).astype(BF16)
             return carry
 
-        lax.fori_loop(0, ROWS // BLOCK, body, 0)
+        lax.fori_loop(0, ROWS // 64, body, 0)
 
     def pair_copy(s, j):
         k = s * NSUB + j
-        return remote(pair_s.at[k], pair_r.at[k], pr_ss.at[k], pr_rs.at[k], dev_pair)
+        return remote(pair_s.at[k], pair_r.at[k], pr_ss, pr_rs.at[k], dev_pair)
 
     def z_copy(s, j):
         k = s * NSUB + j
-        return remote(z_s.at[k], z_r.at[k], z_ss.at[k], z_rs.at[k], dev_up)
+        return remote(z_s.at[k], z_r.at[k], z_ss, z_rs.at[k], dev_up)
 
     def vocab_piece(s, j):
-        away = (1 - 2 * c) * (1 + s)
-        own_dest = lax.rem(z + 2 * NZ - away, NZ) * 2 + c
-        pair_dest = lax.rem(z + 2 * NZ + away, NZ) * 2 + 1 - c
-        both = jnp.concatenate(
-            [normed[:, aligned(dest * CHUNK, CHUNK, CHUNK)] for dest in (own_dest, pair_dest)], axis=1
-        )
-        value = lax.dot_general(
-            both, grads[:, sub_cols(j)], (((0,), (0,)), ((), ())), preferred_element_type=F32
-        )
+        if s == 0:
+            value = jnp.dot(turn_v[...], grads[:, sub_cols(j)], preferred_element_type=F32)
+        else:
+            value = lax.dot_general(
+                vocab_rows(s), grads[:, sub_cols(j)], (((0,), (0,)), ((), ())),
+                preferred_element_type=F32,
+            )
         v_own[(s % 2) * NSUB + j] = value[0:CHUNK]
         pair_s[s * NSUB + j] = value[CHUNK:].astype(BF16)
         pair_copy(s, j).start()
@@ -455,9 +489,15 @@
     z_piece(0, NSUB - 1)
     sent()
 
-    first, middle, finish_a, middle_b, finish_b, sent_rows = rs_tools(
+    first, second, middle, finish_a, middle_b, finish_b, sent_rows = rs_tools(
         rra, rrb, rrc, rsb2, rra2, rrb2, rrc2, rr_ss, rr_rs
     )
+    def drain():
+        sent_rows()
+        gone(normed.at[pl.ds(0, 26 * HALF), :], ag_ss.at[1])
+        gone(stat_r, st_ss)
+        gone(pair_s, pr_ss)
+
     row_order = (far, up, dn, a)
     for s in range(NZ):
 
@@ -474,9 +514,11 @@
         if s == 0:
             first()
         elif s == 2:
+            second(0)
+            second(1)
             middle()
         elif s == 4:
-            finish_a()
+            finish_a(range(RING))
         elif s == 5:
             middle_b()
         elif s == 6:
@@ -490,30 +532,15 @@
             pltpu.make_async_copy(sg_v, sg_o, out_sem.at[NSUB]).start()
             own = jnp.broadcast_to(loss_v[pl.ds(a, 1), :], (8, 128))
             own = pltpu.roll(own, lax.rem(128 - b * BLOCK, 128), 1)
-            loss_o[...] = own[0:1, 0:BLOCK]
-
-    sent_rows()
-    for kind in range(4):
-        gather_b(kind).wait_send()
-        for t in range(RING):
-            gather_a(kind, t).wait_send()
-    for phase in range(2):
-        for k in range(3):
-            stat_copy(phase, k).wait_send()
-
-    def drain_pair(k, carry):
-        pair_copy(0, k).wait_send()
-        return carry
-
-    def drain_z(k, carry):
-        z_copy(0, k).wait_send()
-        return carry
-
-    lax.fori_loop(0, NZ * NSUB, drain_pair, 0)
-    lax.fori_loop(0, (NZ - 1) * NSUB, drain_z, 0)
+            loss_out[...] = own[0:1, 0:BLOCK]
+            pltpu.make_async_copy(loss_out, loss_o, out_sem.at[NSUB + 1]).start()
+            drain()
+
+    gone(z_s, z_ss)
     for j in range(NSUB):
         out_copy(j).wait()
     pltpu.make_async_copy(sg_v, sg_o, out_sem.at[NSUB]).wait()
+    pltpu.make_async_copy(loss_out, loss_o, out_sem.at[NSUB + 1]).wait()
 
 
 def shards(hid, down, res, pg, fg, voc, bias, ids, wts):
@@ -537,8 +564,9 @@
         vmem((1, WIDTH), F32),
         vmem((WIDTH, COLS), BF16),
         vmem((1, COLS), F32),
-        vmem((ROWS, 4), jnp.int32),
-        vmem((ROWS, 4), F32),
+        vmem((4, ROWS), jnp.int32),
+        vmem((4, ROWS), F32),
+        vmem((ROWS, 128), F32),
         vmem((ROWS, WIDTH), BF16),
         vmem((ROWS, COLS), F32),
         vmem((ROWS, COLS), F32),
@@ -549,12 +577,13 @@
         *rs_bufs,
         vmem((4, HALF, WIDTH), F32),
         *rs_bufs,
-        vmem((ROWS, 128), F32),
-        vmem((ROWS, 128), F32),
+        vmem((CHUNK, 128), F32),
+        vmem((2 * CHUNK, ROWS), BF16),
         vmem((ROWS, 128), F32),
         vmem((3, 8, 128), F32),
         vmem((6, 8, 128), F32),
         vmem((RING, 128), F32),
+        vmem((1, BLOCK), F32),
         vmem((2 * NSUB, CHUNK, SUB), F32),
         vmem((NZ * NSUB, CHUNK, SUB), BF16),
         vmem((NZ * NSUB, CHUNK, SUB), BF16),
@@ -563,13 +592,13 @@
         vmem((BLOCK, WIDTH), F32),
         vmem((NSUB, CHUNK, SUB), F32),
         dma((11,)),
-        dma((16,)),
-        dma((NSUB + 1,)),
-        *[dma((30,))] * 4,
-        *[dma((20,))] * 2,
-        *[dma((6,))] * 2,
-        *[dma((NZ * NSUB,))] * 2,
-        *[dma(((NZ - 1) * NSUB,))] * 2,
+        dma(()),
+        dma((NSUB + 2,)),
+        dma(()), dma((11,)), dma(()), dma((11,)),
+        dma((2,)), dma((12,)),
+        dma(()), dma((2,)),
+        dma(()), dma((NZ * NSUB,)),
+        dma(()), dma(((NZ - 1) * NSUB,)),
     ]
     losses, stream_grad, vocab_grad = pl.pallas_call(
         kernel,
@@ -579,13 +608,30 @@
             jax.ShapeDtypeStruct((CHUNK, COLS), F32),
         ),
         in_specs=[hbm] * 9,
-        out_specs=(pl.BlockSpec(memory_space=pltpu.VMEM), pl.BlockSpec(memory_space=pltpu.HBM), pl.BlockSpec(memory_space=pltpu.HBM)),
+        out_specs=(hbm,) * 3,
         scratch_shapes=scratch,
         compiler_params=pltpu.CompilerParams(
             collective_id=0, has_side_effects=True, vmem_limit_bytes=60 * 1024 * 1024
         ),
     )(hid, down, res, pg.reshape(1, WIDTH), fg.reshape(1, WIDTH), voc,
-      bias.reshape(1, COLS), ids, wts)
+      bias.reshape(1, COLS), ids.T, wts.T)
+    blocks = (
+        pl.BlockSpec((1, BLOCK), lambda g: (0, 0)),
+        pl.BlockSpec((BLOCK // 2, WIDTH), lambda g: (g, 0)),
+        pl.BlockSpec((CHUNK // 2, COLS), lambda g: (g, 0)),
+    )
+
+    def place(*refs):
+        for k in range(3):
+            refs[3 + k][...] = refs[k][...]
+
+    losses, stream_grad, vocab_grad = pl.pallas_call(
+        place,
+        grid=(2,),
+        out_shape=tuple(jax.ShapeDtypeStruct(o.shape, o.dtype) for o in (losses, stream_grad, vocab_grad)),
+        in_specs=blocks,
+        out_specs=blocks,
+    )(losses, stream_grad, vocab_grad)
     return losses.reshape(BLOCK), stream_grad, vocab_grad
 
 

time: 121 us -> 103 us (0.85)
  Pallas kernels: 112 us -> 103 us
  local copies, waits for them, and re-layouts: 8.18 us -> 0 us
    pallas_call x1, Pallas kernels: 112 us -> 100 us  [shards(): pl.pallas_call(kernel, out_shape=(jax.ShapeDtypeStruct((1, BLOCK), F32),...]
    unnamed x5 -> x0, local copies, waits for them, and re-layouts: 8.18 us -> none
    pallas_call x0 -> x1, Pallas kernels: none -> 2.23 us  [shards(): pl.pallas_call(place, grid=(2,), out_shape=tuple((jax.ShapeDtypeStruct(o....]
where the time goes in v2:
time: 103 us
  Pallas kernels  103 us (100%)
    pallas_call x1, Pallas kernels, shards(): pl.pallas_call(kernel, out_shape=(jax.ShapeDtypeStruct((1, BLOCK), F32),...  100 us
    pallas_call x1, Pallas kernels, shards(): pl.pallas_call(place, grid=(2,), out_shape=tuple((jax.ShapeDtypeStruct(o....  2.23 us

profile of v2, /device:TPU:2, one launch (start us, length us, event | category | flops | bytes accessed | tf_op | source)
XLA Modules:
  0.0 103.2 jit_solution(6604028778238969070)
XLA Ops:
  0.6 100.3 %shard_map.112 = (f32[1,32]{1,0:T(1,128)}, f32[32,2048]{1,0:T(8,128)}, f32[128,2048]{1,0:T(8,128)}) custom-call(bf16[512,512]{1,0:T(8,128)(2,1)} %hid.1, bf16[512,2048]{1,0:T(8,128)(2,1)} %down.1, bf16[32,2048]{1,0:T(8,128)(2,1)} %res.1, f32[1,2048]{1,0:T(1,128)} %bitcast.6, f32[1,2048]{1,0:T(1,128)} %bitcast.7, bf16[2048,2048]{1,0:T(8,128)(2,1)} %voc.1, ...), custom_call_target="tpu_custom_call" | custom-call | tf_op jit(solution)/shard_map/pallas_call | solution.py:603
  100.9 2.2 %shard_map.113 = (f32[1,32]{1,0:T(1,128)}, f32[32,2048]{1,0:T(8,128)}, f32[128,2048]{1,0:T(8,128)}) custom-call(f32[1,32]{1,0:T(1,128)} %get-tuple-element.9.refs_0_, f32[32,2048]{1,0:T(8,128)} %get-tuple-element.10.refs_1_, f32[128,2048]{1,0:T(8,128)} %get-tuple-element.11.refs_2_), custom_call_target="tpu_custom_call" | custom-call | tf_op jit(solution)/shard_map/pallas_call | solution.py:628

commit v3 on v2

--- a/solution.py
+++ b/solution.py
@@ -44,9 +44,9 @@
     part, scores, wanted, normed, grads, stream_v, inv_v,
     ra, rb, rc, sb2, ra2, rb2, rc2, keep2,
     rra, rrb, rrc, rsb2, rra2, rrb2, rrc2,
-    stat_c, turn_v, norm_c, stat_s, stat_r, loss_v, loss_out,
-    v_own, pair_s, pair_r, z_s, z_r, sg_v, vg_v,
-    load_sem, hid_sem, out_sem,
+    stat_c, turn_v, norm_c, stat_s, stat_r, loss_v,
+    v_own, pair_s, pair_r, z_s, z_r,
+    load_sem, hid_sem,
     rs_ss, rs_rs, rr_ss, rr_rs, ag_ss, ag_rs, st_ss, st_rs, pr_ss, pr_rs, z_ss, z_rs,
 ):
     y, x, z, c = (lax.axis_index(name) for name in AXES)
@@ -56,13 +56,9 @@
     def mod4(value):
         return lax.rem(value, RING)
 
-    def dev_a(step):
-        to = mod4(a + step)
-        return (y + c * (to - y), to + c * (x - to), z, c)
-
-    def dev_b(step):
-        to = mod4(b + step)
-        return (to + c * (y - to), x + c * (to - x), z, c)
+    def dev(step_a, step_b):
+        to_a, to_b = mod4(a + step_a), mod4(b + step_b)
+        return (to_b + c * (to_a - to_b), to_a + c * (to_b - to_a), z, c)
 
     up_z = lax.rem(z + 1 + c * (NZ - 2), NZ)
     down_z = lax.rem(z + NZ - 1 - c * (NZ - 2), NZ)
@@ -97,11 +93,10 @@
     def gone(view, sem):
         remote(view, view, sem, sem, dev_pair).wait_send()
 
-    a_up, a_dn, a_far = dev_a(1), dev_a(3), dev_a(2)
-    b_up, b_dn, b_far = dev_b(1), dev_b(3), dev_b(2)
+    a_up, a_dn, b_up, b_dn = dev(1, 0), dev(3, 0), dev(0, 1), dev(0, 3)
 
     barrier = pltpu.get_barrier_semaphore()
-    for to in (a_up, a_dn, a_far, b_up, b_dn, b_far, dev_pair, dev_down):
+    for to in (a_up, a_dn, b_up, b_dn, dev_pair, dev_down):
         pl.semaphore_signal(barrier, inc=1, device_id=to, device_id_type=MESH)
 
     hid_copies = []
@@ -133,7 +128,8 @@
             value = jnp.dot(
                 hid_v[chunk_rows(i), :], down_v[:, sub_cols(n)], preferred_element_type=F32
             )
-            scores[chunk_rows(i), sub_cols(n)] = value
+            if ready is None:
+                scores[chunk_rows(i), sub_cols(n)] = value
             if send:
                 part[chunk_rows(i), sub_cols(n)] = value.astype(BF16)
             return carry
@@ -175,17 +171,18 @@
             )[kind]
             return remote(src, dst, ss, rs.at[8 + min(kind, 2)], to)
 
-        def first():
-            for t in range(RING):
+        def first(turns):
+            for t in turns:
                 one(0, t).start()
                 one(1, t).start()
 
-        def second(t):
-            one(2, t).start()
-            one(3, t).start()
-
-        def middle():
-            for t in range(RING):
+        def second(turns):
+            for t in turns:
+                one(2, t).start()
+                one(3, t).start()
+
+        def third(turns):
+            for t in turns:
                 q = q_of(t)
                 arrived(ra.at[:, t], rs.at[t])
                 for kind, i, h in ((0, up, 0), (1, dn, 1)):
@@ -193,8 +190,6 @@
                         scores[rows(i, q, h), :] + ra[h, t].astype(F32)
                     ).astype(BF16)
                     one(4 + kind, t).start()
-                if t < 2:
-                    second(t + 2)
 
         def finish_a(turns):
             for t in turns:
@@ -236,7 +231,7 @@
         def sent():
             gone(part.at[pl.ds(0, 30 * HALF), :], ss)
 
-        return first, second, middle, finish_a, middle_b, finish_b, sent
+        return first, second, third, finish_a, middle_b, finish_b, sent
 
     def wanted_block(p):
         i, q = p // RING, lax.rem(p, RING)
@@ -259,21 +254,25 @@
 
         lax.fori_loop(start, stop, body, 0)
 
-    first, second, middle, finish_a, middle_b, finish_b, sent = rs_tools(
+    first, second, third, finish_a, middle_b, finish_b, sent = rs_tools(
         ra, rb, rc, sb2, ra2, rb2, rc2, rs_ss, rs_rs
     )
     pltpu.make_async_copy(hid, hid_v, hid_sem).wait()
     branch_chunk(mod4(a + 2), True, loads[0:4])
     for copy in loads[4:]:
         copy.start()
-    pl.semaphore_wait(barrier, 8)
-    first()
+    pl.semaphore_wait(barrier, 6)
+    first((0, 1, 2))
     branch_chunk(mod4(a + 1), True)
     branch_chunk(mod4(a + 3), True)
-    second(0)
-    second(1)
+    second((0, 1))
     branch_chunk(a, False)
-    middle()
+    third((0,))
+    first((3,))
+    third((1,))
+    second((2,))
+    third((2,))
+    second((3,))
     for copy in loads[4:10]:
         copy.wait()
     for g in range(RING):
@@ -282,6 +281,7 @@
         meta_v[lanes, :] = jnp.transpose(jnp.concatenate([both] * 16, axis=0))
     wanted_blocks(0, 8)
     finish_a((0,))
+    third((3,))
     wanted_blocks(8, 16)
     finish_a((1, 2))
     middle_b()
@@ -297,103 +297,119 @@
     up, dn, far = mod4(a + 1), mod4(a + 3), mod4(a + 2)
     b1, b3, b2 = mod4(b + 1), mod4(b + 3), mod4(b + 2)
 
-    def gather_b(kind, arriving=False):
+    def gather_b(kind):
         at, to = (
-            (rows32(a, b3 if arriving else b), b_up),
-            (rows32(a, b1 if arriving else b), b_dn),
-            (rows(a, b2 if arriving else b3, 0), b_up),
-            (rows(a, b2 if arriving else b1, 1), b_dn),
+            (rows(a, b, 0), b_up),
+            (rows(a, b, 1), b_dn),
+            (rows(a, b, 1), b_up),
+            (rows(a, b, 0), b_dn),
+            (rows(a, b3, 0), b_up),
+            (rows(a, b1, 1), b_dn),
         )[kind]
-        return remote(
-            normed.at[at, :], normed.at[at, :], ag_ss.at[kind // 2], ag_rs.at[min(kind, 2)], to
-        )
-
-    def gather_a(kind, t, arriving=False):
+        send, recv = ((0, 0), (0, 1), (0, 2), (0, 2), (1, 3), (1, 3))[kind]
+        return remote(normed.at[at, :], normed.at[at, :], ag_ss.at[send], ag_rs.at[recv], to)
+
+    def gather_a(kind, t):
         q = mod4(b + AG_ORDER[t])
         at, to = (
-            (rows32(dn if arriving else a, q), a_up),
-            (rows32(up if arriving else a, q), a_dn),
-            (rows(far if arriving else dn, q, 0), a_up),
-            (rows(far if arriving else up, q, 1), a_dn),
+            (rows32(a, q), a_up),
+            (rows32(a, q), a_dn),
+            (rows(dn, q, 0), a_up),
+            (rows(up, q, 1), a_dn),
+            (rows(a, q, 0), a_up),
+            (rows(a, q, 1), a_dn),
+            (rows(a, q, 1), a_up),
+            (rows(a, q, 0), a_dn),
         )[kind]
-        recv = ag_rs.at[3 + 2 * t + kind if kind < 2 else 11]
+        recv = ag_rs.at[(4 + 2 * t, 5 + 2 * t, 12, 12, 10, 11, 13, 13)[kind]]
         return remote(normed.at[at, :], normed.at[at, :], ag_ss.at[1], recv, to)
 
     def forward_a(t):
+        q = mod4(b + AG_ORDER[t])
+        for kind, i in ((0, dn), (1, up)):
+            at = rows32(i, q) if t < 3 else rows(i, q, kind)
+            arrived(normed.at[at, :], ag_rs.at[4 + 2 * t + kind])
+            gather_a(2 + kind, t).start()
+
+    for kind in range(4):
+        gather_b(kind).start()
+
+    def first_a():
+        gone(normed.at[pl.ds(0, 2 * BLOCK), :], ag_ss.at[0])
         for kind in (0, 1):
-            gather_a(kind, t, True).wait_recv()
-            gather_a(2 + kind, t).start()
-
-    for kind in (0, 1):
-        gather_b(kind).start()
-    gone(normed.at[pl.ds(0, 2 * BLOCK), :], ag_ss.at[0])
-    for kind in (0, 1):
-        gather_a(kind, 0).start()
-    for kind in (0, 1):
-        gather_b(kind, True).wait_recv()
-        gather_b(2 + kind).start()
+            gather_a(kind, 0).start()
+
+    pl.when(c == 0)(first_a)
+    for kind, q in ((0, b3), (1, b1)):
+        arrived(normed.at[rows(a, q, kind), :], ag_rs.at[kind])
+        gather_b(4 + kind).start()
+    pl.when(c == 1)(first_a)
+    arrived(normed.at[pl.ds(0, BLOCK), :], ag_rs.at[2])
     for kind in (0, 1):
         gather_a(0, 1 + kind).start()
         gather_a(1, 1 + kind).start()
     forward_a(0)
-    arrived(normed.at[rows32(a, b2), :], ag_rs.at[2])
-    for kind in (0, 1):
+    arrived(normed.at[rows32(a, b2), :], ag_rs.at[3])
+    for kind in (4, 5, 6, 7):
         gather_a(kind, 3).start()
     pltpu.make_async_copy(voc, voc_v, load_sem.at[10]).wait()
 
-    def score_pieces(chunks, start, stop):
+    def score_pieces(places, start, stop):
         def piece(n, carry):
-            rows_in = [normed[chunk_rows(i), :] for i in chunks]
+            rows_in = [normed[at, :] for at in places]
             value = jnp.dot(
                 jnp.concatenate(rows_in, axis=0), voc_v[:, sub_cols(n)], preferred_element_type=F32
             ) + bias_v[:, sub_cols(n)]
-            for k, i in enumerate(chunks):
-                scores[chunk_rows(i), sub_cols(n)] = value[k * CHUNK : (k + 1) * CHUNK]
+            first_row = 0
+            for at in places:
+                scores[at, sub_cols(n)] = value[first_row : first_row + at.size]
+                first_row += at.size
             return carry
 
         lax.fori_loop(start, stop, piece, 0)
 
-    first_lane = lax.broadcasted_iota(jnp.int32, (64, 128), 1) == 0
-
-    def stats(i):
-        for r in range(2):
-            at = aligned(i * CHUNK + r * 64, 64, 64)
-            groups = [pl.ds(g * 128, 128) for g in range(COLS // 128)]
+    def stats(places):
+        groups = [pl.ds(g * 128, 128) for g in range(COLS // 128)]
+        for at in places:
             peak = scores[at, groups[0]]
             for group in groups[1:]:
                 peak = jnp.maximum(peak, scores[at, group])
-            peak = jnp.broadcast_to(jnp.max(peak, axis=1, keepdims=True), (64, 128))
-            total = jnp.zeros((64, 128), F32)
-            target = jnp.zeros((64, 128), F32)
+            peak = jnp.broadcast_to(jnp.max(peak, axis=1, keepdims=True), (at.size, 128))
+            total = jnp.zeros((at.size, 128), F32)
+            target = jnp.zeros((at.size, 128), F32)
             for group in groups:
                 value = scores[at, group]
                 total = total + jnp.exp(value - peak)
                 target = target + wanted[at, group] * value
             lse = peak + jnp.log(jnp.sum(total, axis=1, keepdims=True))
-            stat_c[pl.ds(r * 64, 64), :] = jnp.where(
-                first_lane, lse, jnp.sum(target, axis=1, keepdims=True)
-            )
-        turned = jnp.transpose(stat_c[...])
-        stat_s[0, pl.ds(i, 1), :] = turned[0:1, :]
-        stat_s[0, pl.ds(i + RING, 1), :] = turned[1:2, :]
-
-    score_pieces((a,), 0, 2)
+            first_lane = lax.broadcasted_iota(jnp.int32, (at.size, 128), 1) == 0
+            stat_c[at, :] = jnp.where(first_lane, lse, jnp.sum(target, axis=1, keepdims=True))
+
+    def rows64(i):
+        return [aligned(i * CHUNK + r * 64, 64, 64) for r in range(2)]
+
+    early = [rows32(i, mod4(b + AG_ORDER[t])) for i in (up, dn) for t in range(3)]
+    late = [rows32(up, b2), rows32(dn, b2)]
+    score_pieces([chunk_rows(a)], 0, 2)
     forward_a(1)
-    score_pieces((a,), 2, 4)
+    score_pieces([chunk_rows(a)], 2, 4)
     forward_a(2)
-    stats(a)
+    score_pieces(early, 0, 2)
     forward_a(3)
-    score_pieces((up, dn), 0, 4)
-    stats(up)
-    stats(dn)
-    arrived(normed.at[chunk_rows(far), :], ag_rs.at[11])
-    score_pieces((far,), 0, 4)
-    stats(far)
-
-    def stat_copy(phase, k):
-        to = ((a_up, a_dn, a_far), (b_up, b_dn, b_far))[phase][k]
-        n = phase * 3 + k
-        return remote(stat_s.at[phase], stat_r.at[n], st_ss, st_rs.at[phase], to)
+    score_pieces(early, 2, 4)
+    stats(rows64(a))
+    stats(early)
+    arrived(normed.at[rows32(a, b), :], ag_rs.at[13])
+    arrived(normed.at[chunk_rows(far), :], ag_rs.at[12])
+    score_pieces(late + [chunk_rows(far)], 0, 4)
+    stats(late + rows64(far))
+    for i in range(RING):
+        turned = jnp.transpose(stat_c[pl.ds(i * CHUNK, CHUNK), :])
+        stat_s[0, i : i + 1, :] = turned[0:1, :]
+        stat_s[0, i + RING : i + RING + 1, :] = turned[1:2, :]
+
+    def stat_copy(k):
+        return remote(stat_s.at[0], stat_r.at[k], st_ss, st_rs, dev(k // RING, k % RING))
 
     def vocab_rows(s):
         away = (1 - 2 * c) * (1 + s)
@@ -404,22 +420,22 @@
         )
 
     is_lse = lax.broadcasted_iota(jnp.int32, (8, 128), 0) < RING
-    for phase in range(2):
-        for k in range(3):
-            stat_copy(phase, k).start()
-        if phase == 0:
-            turn_v[...] = jnp.transpose(vocab_rows(0))
-        arrived(stat_r.at[pl.ds(phase * 3, 3)], st_rs.at[phase])
-        parts = [stat_s[phase]] + [stat_r[phase * 3 + k] for k in range(3)]
-        peak = jnp.maximum(jnp.maximum(parts[0], parts[1]), jnp.maximum(parts[2], parts[3]))
-        joint = peak + jnp.log(sum(jnp.exp(value - peak) for value in parts))
-        stat_s[phase + 1] = jnp.where(is_lse, joint, sum(parts))
-    log_rows = stat_s[2, 0:RING, :]
+    for k in (10, 9, 11, 6, 14, 5, 7, 13, 15, 2, 8, 1, 3, 4, 12):
+        stat_copy(k).start()
+    turn_v[...] = jnp.transpose(vocab_rows(0))
+    arrived(stat_r.at[pl.ds(1, 15)], st_rs)
+    parts = [stat_s[0]] + [stat_r[k] for k in range(1, 16)]
+    peak = parts[0]
+    for value in parts[1:]:
+        peak = jnp.maximum(peak, value)
+    joint = peak + jnp.log(sum(jnp.exp(value - peak) for value in parts))
+    stat_s[1] = jnp.where(is_lse, joint, sum(parts))
+    log_rows = stat_s[1, 0:RING, :]
     for i in range(RING):
         norm_c[pl.ds(i * CHUNK, CHUNK), :] = jnp.transpose(
-            jnp.broadcast_to(stat_s[2, i : i + 1, :], (CHUNK, 128))
+            jnp.broadcast_to(stat_s[1, i : i + 1, :], (CHUNK, 128))
         )
-    loss_v[...] = log_rows - stat_s[2, RING:8, :] + Z_WEIGHT * log_rows * log_rows
+    loss_v[...] = log_rows - stat_s[1, RING:8, :] + Z_WEIGHT * log_rows * log_rows
 
     def grad_block(j):
         def body(r, carry):
@@ -467,11 +483,7 @@
             z_s[k] = value.astype(BF16)
             z_copy(s, j).start()
         else:
-            vg_v[j] = value
-            out_copy(j).start()
-
-    def out_copy(j):
-        return pltpu.make_async_copy(vg_v.at[j], vg_o.at[:, sub_cols(j)], out_sem.at[j])
+            vg_o[:, sub_cols(j)] = value
 
     def row_piece(i, n):
         value = lax.dot_general(
@@ -489,13 +501,13 @@
     z_piece(0, NSUB - 1)
     sent()
 
-    first, second, middle, finish_a, middle_b, finish_b, sent_rows = rs_tools(
+    first, second, third, finish_a, middle_b, finish_b, sent_rows = rs_tools(
         rra, rrb, rrc, rsb2, rra2, rrb2, rrc2, rr_ss, rr_rs
     )
     def drain():
         sent_rows()
         gone(normed.at[pl.ds(0, 26 * HALF), :], ag_ss.at[1])
-        gone(stat_r, st_ss)
+        gone(stat_r.at[pl.ds(1, 15)], st_ss)
         gone(pair_s, pr_ss)
 
     row_order = (far, up, dn, a)
@@ -512,11 +524,14 @@
 
         lax.fori_loop(0, NSUB, slot, 0)
         if s == 0:
-            first()
+            first(range(RING))
         elif s == 2:
-            second(0)
-            second(1)
-            middle()
+            second((0, 1))
+            third((0,))
+            second((2,))
+            third((1,))
+            second((3,))
+            third((2, 3))
         elif s == 4:
             finish_a(range(RING))
         elif s == 5:
@@ -525,22 +540,16 @@
             stream = stream_v[...]
             inverse = inv_v[:, 0:1]
             upstream = finish_b() * fg_v[...]
-            sg_v[...] = inverse * (
+            sg_o[...] = inverse * (
                 upstream
                 - stream * inverse * inverse * jnp.mean(upstream * stream, axis=-1, keepdims=True)
             )
-            pltpu.make_async_copy(sg_v, sg_o, out_sem.at[NSUB]).start()
             own = jnp.broadcast_to(loss_v[pl.ds(a, 1), :], (8, 128))
             own = pltpu.roll(own, lax.rem(128 - b * BLOCK, 128), 1)
-            loss_out[...] = own[0:1, 0:BLOCK]
-            pltpu.make_async_copy(loss_out, loss_o, out_sem.at[NSUB + 1]).start()
+            loss_o[...] = own[0:1, 0:BLOCK]
             drain()
 
     gone(z_s, z_ss)
-    for j in range(NSUB):
-        out_copy(j).wait()
-    pltpu.make_async_copy(sg_v, sg_o, out_sem.at[NSUB]).wait()
-    pltpu.make_async_copy(loss_out, loss_o, out_sem.at[NSUB + 1]).wait()
 
 
 def shards(hid, down, res, pg, fg, voc, bias, ids, wts):
@@ -577,61 +586,40 @@
         *rs_bufs,
         vmem((4, HALF, WIDTH), F32),
         *rs_bufs,
-        vmem((CHUNK, 128), F32),
+        vmem((ROWS, 128), F32),
         vmem((2 * CHUNK, ROWS), BF16),
         vmem((ROWS, 128), F32),
-        vmem((3, 8, 128), F32),
-        vmem((6, 8, 128), F32),
+        vmem((2, 8, 128), F32),
+        vmem((16, 8, 128), F32),
         vmem((RING, 128), F32),
-        vmem((1, BLOCK), F32),
         vmem((2 * NSUB, CHUNK, SUB), F32),
         vmem((NZ * NSUB, CHUNK, SUB), BF16),
         vmem((NZ * NSUB, CHUNK, SUB), BF16),
         vmem(((NZ - 1) * NSUB, CHUNK, SUB), BF16),
         vmem(((NZ - 1) * NSUB, CHUNK, SUB), BF16),
-        vmem((BLOCK, WIDTH), F32),
-        vmem((NSUB, CHUNK, SUB), F32),
         dma((11,)),
         dma(()),
-        dma((NSUB + 2,)),
         dma(()), dma((11,)), dma(()), dma((11,)),
-        dma((2,)), dma((12,)),
-        dma(()), dma((2,)),
+        dma((2,)), dma((14,)),
+        dma(()), dma(()),
         dma(()), dma((NZ * NSUB,)),
         dma(()), dma(((NZ - 1) * NSUB,)),
     ]
     losses, stream_grad, vocab_grad = pl.pallas_call(
         kernel,
         out_shape=(
-            jax.ShapeDtypeStruct((1, BLOCK), F32),
-            jax.ShapeDtypeStruct((BLOCK, WIDTH), F32),
-            jax.ShapeDtypeStruct((CHUNK, COLS), F32),
+            pltpu.VMEM((1, BLOCK), F32),
+            pltpu.VMEM((BLOCK, WIDTH), F32),
+            pltpu.VMEM((CHUNK, COLS), F32),
         ),
         in_specs=[hbm] * 9,
-        out_specs=(hbm,) * 3,
+        out_specs=(pl.BlockSpec(memory_space=pltpu.VMEM),) * 3,
         scratch_shapes=scratch,
         compiler_params=pltpu.CompilerParams(
             collective_id=0, has_side_effects=True, vmem_limit_bytes=60 * 1024 * 1024
         ),
     )(hid, down, res, pg.reshape(1, WIDTH), fg.reshape(1, WIDTH), voc,
       bias.reshape(1, COLS), ids.T, wts.T)
-    blocks = (
-        pl.BlockSpec((1, BLOCK), lambda g: (0, 0)),
-        pl.BlockSpec((BLOCK // 2, WIDTH), lambda g: (g, 0)),
-        pl.BlockSpec((CHUNK // 2, COLS), lambda g: (g, 0)),
-    )
-
-    def place(*refs):
-        for k in range(3):
-            refs[3 + k][...] = refs[k][...]
-
-    losses, stream_grad, vocab_grad = pl.pallas_call(
-        place,
-        grid=(2,),
-        out_shape=tuple(jax.ShapeDtypeStruct(o.shape, o.dtype) for o in (losses, stream_grad, vocab_grad)),
-        in_specs=blocks,
-        out_specs=blocks,
-    )(losses, stream_grad, vocab_grad)
     return losses.reshape(BLOCK), stream_grad, vocab_grad
 
 

time: 103 us -> 99.4 us (0.965)
  Pallas kernels: 103 us -> 96.5 us
  local copies, waits for them, and re-layouts: 0 us -> 2.18 us
    pallas_call x2 -> x1, Pallas kernels: 103 us -> 96.5 us  [shards(): pl.pallas_call(kernel, out_shape=(pltpu.VMEM((1, BLOCK), F32), pltpu.VMEM...]
    unnamed x0 -> x3, local copies, waits for them, and re-layouts: none -> 2.18 us
where the time goes in v3:
time: 99.4 us; the launch traced here: 99.3 us
  Pallas kernels  96.5 us (97%)
  local copies, waits for them, and re-layouts  2.18 us (2%)
    pallas_call x1, Pallas kernels, shards(): pl.pallas_call(kernel, out_shape=(pltpu.VMEM((1, BLOCK), F32), pltpu.VMEM...  96.5 us
    unnamed x3, local copies, waits for them, and re-layouts  2.18 us

profile of v3, /device:TPU:2, one launch (start us, length us, event | category | flops | bytes accessed | tf_op | source)
XLA Modules:
  0.0 99.3 jit_solution(11700946534561484750)
XLA Ops:
  0.6 96.5 %shard_map.112 = (f32[1,32]{1,0:T(1,128)S(1)}, f32[32,2048]{1,0:T(8,128)S(1)}, f32[128,2048]{1,0:T(8,128)S(1)}) custom-call(bf16[512,512]{1,0:T(8,128)(2,1)} %hid.1, bf16[512,2048]{1,0:T(8,128)(2,1)} %down.1, bf16[32,2048]{1,0:T(8,128)(2,1)} %res.1, f32[1,2048]{1,0:T(1,128)} %bitcast.7, f32[1,2048]{1,0:T(1,128)} %bitcast.8, bf16[2048,2048]{1,0:T(8,128)(2,1)} %voc.1, ...), custom_call_target="tpu_custom_call" | custom-call | tf_op jit(solution)/shard_map/pallas_call | solution.py:608
  97.1 0.5 copy.15
  97.7 0.7 copy.16
  98.4 1.0 copy.17

commit v4 on v3

--- a/solution.py
+++ b/solution.py
@@ -267,11 +267,10 @@
     branch_chunk(mod4(a + 3), True)
     second((0, 1))
     branch_chunk(a, False)
-    third((0,))
-    first((3,))
-    third((1,))
+    third((0, 1))
     second((2,))
     third((2,))
+    first((3,))
     second((3,))
     for copy in loads[4:10]:
         copy.wait()
@@ -281,10 +280,10 @@
         meta_v[lanes, :] = jnp.transpose(jnp.concatenate([both] * 16, axis=0))
     wanted_blocks(0, 8)
     finish_a((0,))
-    third((3,))
     wanted_blocks(8, 16)
     finish_a((1, 2))
     middle_b()
+    third((3,))
     finish_a((3,))
     branch = finish_b()
 
@@ -306,8 +305,8 @@
             (rows(a, b3, 0), b_up),
             (rows(a, b1, 1), b_dn),
         )[kind]
-        send, recv = ((0, 0), (0, 1), (0, 2), (0, 2), (1, 3), (1, 3))[kind]
-        return remote(normed.at[at, :], normed.at[at, :], ag_ss.at[send], ag_rs.at[recv], to)
+        recv = ag_rs.at[(0, 1, 2, 2, 3, 3)[kind]]
+        return remote(normed.at[at, :], normed.at[at, :], ag_ss, recv, to)
 
     def gather_a(kind, t):
         q = mod4(b + AG_ORDER[t])
@@ -322,7 +321,7 @@
             (rows(a, q, 0), a_dn),
         )[kind]
         recv = ag_rs.at[(4 + 2 * t, 5 + 2 * t, 12, 12, 10, 11, 13, 13)[kind]]
-        return remote(normed.at[at, :], normed.at[at, :], ag_ss.at[1], recv, to)
+        return remote(normed.at[at, :], normed.at[at, :], ag_ss, recv, to)
 
     def forward_a(t):
         q = mod4(b + AG_ORDER[t])
@@ -334,24 +333,32 @@
     for kind in range(4):
         gather_b(kind).start()
 
-    def first_a():
-        gone(normed.at[pl.ds(0, 2 * BLOCK), :], ag_ss.at[0])
-        for kind in (0, 1):
-            gather_a(kind, 0).start()
-
-    pl.when(c == 0)(first_a)
+    for kind in (0, 1):
+        gather_a(kind, 0).start()
     for kind, q in ((0, b3), (1, b1)):
         arrived(normed.at[rows(a, q, kind), :], ag_rs.at[kind])
         gather_b(4 + kind).start()
-    pl.when(c == 1)(first_a)
     arrived(normed.at[pl.ds(0, BLOCK), :], ag_rs.at[2])
-    for kind in (0, 1):
-        gather_a(0, 1 + kind).start()
-        gather_a(1, 1 + kind).start()
-    forward_a(0)
+
+    def second_a():
+        for t in (1, 2):
+            for kind in (0, 1):
+                gather_a(kind, t).start()
+
+    @pl.when(c == 0)
+    def _():
+        second_a()
+        forward_a(0)
+
     arrived(normed.at[rows32(a, b2), :], ag_rs.at[3])
+    pl.when(c == 1)(second_a)
     for kind in (4, 5, 6, 7):
         gather_a(kind, 3).start()
+
+    @pl.when(c == 1)
+    def _():
+        forward_a(0)
+
     pltpu.make_async_copy(voc, voc_v, load_sem.at[10]).wait()
 
     def score_pieces(places, start, stop):
@@ -506,7 +513,7 @@
     )
     def drain():
         sent_rows()
-        gone(normed.at[pl.ds(0, 26 * HALF), :], ag_ss.at[1])
+        gone(normed.at[pl.ds(0, 30 * HALF), :], ag_ss)
         gone(stat_r.at[pl.ds(1, 15)], st_ss)
         gone(pair_s, pr_ss)
 
@@ -600,7 +607,7 @@
         dma((11,)),
         dma(()),
         dma(()), dma((11,)), dma(()), dma((11,)),
-        dma((2,)), dma((14,)),
+        dma(()), dma((14,)),
         dma(()), dma(()),
         dma(()), dma((NZ * NSUB,)),
         dma(()), dma(((NZ - 1) * NSUB,)),

time: 99.4 us -> 98.2 us (0.988)
  Pallas kernels: 96.5 us -> 95.2 us
    pallas_call x1, Pallas kernels: 96.5 us -> 95.2 us  [shards(): pl.pallas_call(kernel, out_shape=(pltpu.VMEM((1, BLOCK), F32), pltpu.VMEM...]
where the time goes in v4:
time: 98.2 us; the launch traced here: 98.1 us
  Pallas kernels  95.2 us (97%)
  local copies, waits for them, and re-layouts  2.18 us (2%)
    pallas_call x1, Pallas kernels, shards(): pl.pallas_call(kernel, out_shape=(pltpu.VMEM((1, BLOCK), F32), pltpu.VMEM...  95.2 us
    unnamed x3, local copies, waits for them, and re-layouts  2.18 us

profile of v4, /device:TPU:2, one launch (start us, length us, event | category | flops | bytes accessed | tf_op | source)
XLA Modules:
  0.0 98.1 jit_solution(1932018813786464713)
XLA Ops:
  0.6 95.2 %shard_map.112 = (f32[1,32]{1,0:T(1,128)S(1)}, f32[32,2048]{1,0:T(8,128)S(1)}, f32[128,2048]{1,0:T(8,128)S(1)}) custom-call(bf16[512,512]{1,0:T(8,128)(2,1)} %hid.1, bf16[512,2048]{1,0:T(8,128)(2,1)} %down.1, bf16[32,2048]{1,0:T(8,128)(2,1)} %res.1, f32[1,2048]{1,0:T(1,128)} %bitcast.7, f32[1,2048]{1,0:T(1,128)} %bitcast.8, bf16[2048,2048]{1,0:T(8,128)(2,1)} %voc.1, ...), custom_call_target="tpu_custom_call" | custom-call | tf_op jit(solution)/shard_map/pallas_call | solution.py:615
  95.9 0.5 copy.15
  96.4 0.7 copy.16
  97.1 1.0 copy.17

commit v5 on v4

--- a/solution.py
+++ b/solution.py
@@ -80,6 +80,9 @@
 
     def sub_cols(j):
         return aligned(j * SUB, SUB, SUB)
+
+    def wide_cols(j):
+        return aligned(j * 2 * SUB, 2 * SUB, 2 * SUB)
 
     def remote(src, dst, send, recv, to):
         return pltpu.make_async_remote_copy(
@@ -281,9 +284,10 @@
     wanted_blocks(0, 8)
     finish_a((0,))
     wanted_blocks(8, 16)
-    finish_a((1, 2))
+    finish_a((1,))
+    third((3,))
+    finish_a((2,))
     middle_b()
-    third((3,))
     finish_a((3,))
     branch = finish_b()
 
@@ -365,11 +369,11 @@
         def piece(n, carry):
             rows_in = [normed[at, :] for at in places]
             value = jnp.dot(
-                jnp.concatenate(rows_in, axis=0), voc_v[:, sub_cols(n)], preferred_element_type=F32
-            ) + bias_v[:, sub_cols(n)]
+                jnp.concatenate(rows_in, axis=0), voc_v[:, wide_cols(n)], preferred_element_type=F32
+            ) + bias_v[:, wide_cols(n)]
             first_row = 0
             for at in places:
-                scores[at, sub_cols(n)] = value[first_row : first_row + at.size]
+                scores[at, wide_cols(n)] = value[first_row : first_row + at.size]
                 first_row += at.size
             return carry
 
@@ -397,18 +401,18 @@
 
     early = [rows32(i, mod4(b + AG_ORDER[t])) for i in (up, dn) for t in range(3)]
     late = [rows32(up, b2), rows32(dn, b2)]
-    score_pieces([chunk_rows(a)], 0, 2)
+    score_pieces([chunk_rows(a)], 0, 1)
     forward_a(1)
-    score_pieces([chunk_rows(a)], 2, 4)
+    score_pieces([chunk_rows(a)], 1, 2)
     forward_a(2)
-    score_pieces(early, 0, 2)
+    score_pieces(early, 0, 1)
     forward_a(3)
-    score_pieces(early, 2, 4)
+    score_pieces(early, 1, 2)
     stats(rows64(a))
     stats(early)
     arrived(normed.at[rows32(a, b), :], ag_rs.at[13])
     arrived(normed.at[chunk_rows(far), :], ag_rs.at[12])
-    score_pieces(late + [chunk_rows(far)], 0, 4)
+    score_pieces(late + [chunk_rows(far)], 0, 2)
     stats(late + rows64(far))
     for i in range(RING):
         turned = jnp.transpose(stat_c[pl.ds(i * CHUNK, CHUNK), :])

time: 98.2 us -> 97.9 us (level)
  no operation moved by 1% of the time
where the time goes in v5:
time: 97.9 us; the launch traced here: 97.7 us
  Pallas kernels  94.9 us (97%)
  local copies, waits for them, and re-layouts  2.18 us (2%)
    pallas_call x1, Pallas kernels, shards(): pl.pallas_call(kernel, out_shape=(pltpu.VMEM((1, BLOCK), F32), pltpu.VMEM...  94.9 us
    unnamed x3, local copies, waits for them, and re-layouts  2.18 us

profile of v5, /device:TPU:2, one launch (start us, length us, event | category | flops | bytes accessed | tf_op | source)
XLA Modules:
  0.0 97.7 jit_solution(18068337560242881129)
XLA Ops:
  0.6 94.9 %shard_map.112 = (f32[1,32]{1,0:T(1,128)S(1)}, f32[32,2048]{1,0:T(8,128)S(1)}, f32[128,2048]{1,0:T(8,128)S(1)}) custom-call(bf16[512,512]{1,0:T(8,128)(2,1)} %hid.1, bf16[512,2048]{1,0:T(8,128)(2,1)} %down.1, bf16[32,2048]{1,0:T(8,128)(2,1)} %res.1, f32[1,2048]{1,0:T(1,128)} %bitcast.7, f32[1,2048]{1,0:T(1,128)} %bitcast.8, bf16[2048,2048]{1,0:T(8,128)(2,1)} %voc.1, ...), custom_call_target="tpu_custom_call" | custom-call | tf_op jit(solution)/shard_map/pallas_call | solution.py:619
  95.5 0.5 copy.15
  96.0 0.7 copy.16
  96.7 1.0 copy.17
